TPU v7x, 32 devices: a whole 2x2x4 slice. The times are simulated.
32 devices in a mesh: sp: 4 (over z), fs: 4 (over y, x), tp: 2 (over core).
Axes of the slice: x: 2, y: 2, z: 4, core: 2. Of those that a mesh axis runs over, the one named last changes fastest.
Arguments:
- tokens: bfloat16 [4, 1536, 2048], P('fs', ('sp', 'tp')), may hold values from -6 to 6
- norm_gain: float32 [2048], replicated, may hold values from 0.1 to 1.9
- conv_gate_w: bfloat16 [2048, 1024], P('sp', 'tp'), may hold values from -0.125 to 0.125
- conv_in_w: bfloat16 [2048, 1024], P('sp', 'tp'), may hold values from -0.125 to 0.125
- query_w: bfloat16 [2048, 1024], P('sp', 'tp'), may hold values from -0.125 to 0.125
- forget_w: bfloat16 [2048, 1024], P('sp', 'tp'), may hold values from -0.125 to 0.125
- value_w: bfloat16 [2048, 1024], P('sp', 'tp'), may hold values from -0.125 to 0.125
- conv_taps: float32 [3, 1024], P(None, 'tp'), may hold values from -3.5 to 3.5
- floor_gate: float32 [1024], P('tp'), may hold values from 0.93 to 1
- leak: float32 [4, 1536, 8], P('fs', 'sp', 'tp'), may hold values from -1.4 to 0
- head_gain: float32 [128], replicated, may hold values from 0.1 to 1.9
- conv_out_w: bfloat16 [1024, 2048], P('tp', 'fs'), may hold values from -0.125 to 0.125
- chain_out_w: bfloat16 [1024, 2048], P('tp', 'fs'), may hold values from -0.125 to 0.125
Outputs:
- mixed: bfloat16 [4, 1536, 2048], P('fs', ('sp', 'tp'))
All inputs are finite; a program needn't handle non-finite values.
Results may differ from a plain program's by a relative error of at most 0.013.
Values may be sent and summed in bfloat16 or wider, within the bound.
A program may use at most 128 MiB of HBM per device.

v0:
```python
import functools

import jax
import jax.numpy as jnp
from jax import lax
from jax.experimental import pallas as pl
from jax.experimental.pallas import tpu as pltpu
from jax.sharding import PartitionSpec as P

MESH = pl.DeviceIdType.MESH
BF = jnp.bfloat16
F32 = jnp.float32
NT = (((1,), (1,)), ((), ()))
TN = (((0,), (0,)), ((), ()))
GATE, SIGNAL, QUERY, FORGET, VALUE = 4, 3, 1, 0, 2


def kernel(
    ns, nf,
    tok, gain, w0, w1, w2, w3, w4, taps, floor, leak, leak_t, hgain, cow, how,
    out,
    rows, wg, psend, prev, wo, rim, inside, reach, states, sdecay, sin, sout,
    lcol, lrow, mix, osend, orecv, through,
    zs, zsl, zr, zloc, rs, rr, ts, tr, ps, pr, os_, or_, oloc, ms, mr, ss, sr, es, er, ds, dr, ns_, nr,
):
    s, f, t = lax.axis_index("sp"), lax.axis_index("fs"), lax.axis_index("tp")
    other = 1 - t
    half = tok.shape[1]
    length = 2 * half
    kd = w0.shape[0]
    wide = w0.shape[1] // nf
    ws = (w3, w2, w4, w1, w0)
    np_ = len(ws)
    has_left, has_right = s > 0, s < ns - 1

    barrier = pltpu.get_barrier_semaphore()
    pl.semaphore_signal(barrier, inc=1, device_id={"tp": other}, device_id_type=MESH)
    for d in range(1, nf):
        pl.semaphore_signal(barrier, inc=1, device_id={"fs": f ^ d}, device_id_type=MESH)

    @pl.when(has_left)
    def _():
        pl.semaphore_signal(barrier, inc=1, device_id={"sp": s - 1}, device_id_type=MESH)

    @pl.when(has_right)
    def _():
        pl.semaphore_signal(barrier, inc=1, device_id={"sp": s + 1}, device_id_type=MESH)

    ends = jnp.where(has_left, 1, 0) + jnp.where(has_right, 1, 0)
    pl.semaphore_wait(barrier, nf + ends)

    def remote(src, dst, send, recv, **where):
        return pltpu.make_async_remote_copy(
            src_ref=src, dst_ref=dst, send_sem=send, recv_sem=recv,
            device_id=where, device_id_type=MESH,
        )

    def wblock(b, p):
        return wg.at[p, pl.ds(pl.multiple_of(b * kd, kd), kd), :]

    def wown(p):
        return ws[p].at[:, pl.ds(pl.multiple_of(f * wide, wide), wide)]

    def own_right(p):
        return remote(wown(p), wblock(s, p), zs.at[s, p], zr.at[s, p], sp=s + 1)

    def own_left(p):
        return remote(wown(p), wblock(s, p), zsl.at[p], zr.at[s, p], sp=s - 1)

    def relay(b, p, to):
        return remote(wblock(b, p), wblock(b, p), zs.at[b, p], zr.at[b, p], sp=to)

    def send_own(p):
        @pl.when(has_right)
        def _():
            own_right(p).start()

        @pl.when(has_left)
        def _():
            own_left(p).start()

        pltpu.make_async_copy(wown(p), wblock(s, p), zloc.at[p]).start()

    def zrelay(p):
        def hop(k, carry):
            @pl.when(s - k >= 0)
            def _():
                relay(s - k, p, s + 1).wait_recv()

                @pl.when(has_right)
                def _():
                    relay(s - k, p, s + 1).start()

            @pl.when(s + k < ns)
            def _():
                relay(s + k, p, s - 1).wait_recv()

                @pl.when(has_left)
                def _():
                    relay(s + k, p, s - 1).start()

            return carry

        lax.fori_loop(1, ns, hop, 0)
        pltpu.make_async_copy(wown(p), wblock(s, p), zloc.at[p]).wait()
        if p + 2 < np_:
            send_own(p + 2)

    send_own(0)
    send_own(1)

    x = tok[0].astype(F32)
    center = x - jnp.mean(x, axis=-1, keepdims=True)
    spread = jnp.mean(center * center, axis=-1, keepdims=True)
    rows[f, pl.ds(pl.multiple_of(t * half, half), half), :] = (
        center * lax.rsqrt(spread + 1e-05) * gain[...]
    ).astype(BF)

    quarter = half // 2

    def piece(g, j):
        return rows.at[g, pl.ds(pl.multiple_of(t * half + j * quarter, quarter), quarter), :]

    def core_rows(g, core):
        return rows.at[g, pl.ds(pl.multiple_of(core * half, half), half), :]

    def row_arrived(d, j):
        g = f ^ d
        remote(piece(g, j), piece(g, j), rs.at[0], rr.at[d, j], fs=f ^ 1).wait_recv()

    def row_send(d, j, to_d, slot):
        g = f ^ d
        to = f ^ to_d
        return remote(piece(g, j), piece(g, j), rs.at[slot], rr.at[d ^ to_d, j], fs=to)

    def twin(d):
        g = f ^ d
        return remote(core_rows(g, t), core_rows(g, t), ts.at[d], tr.at[d], tp=other)

    def twin_arrived(d):
        g = f ^ d
        remote(core_rows(g, other), core_rows(g, other), ts.at[d], tr.at[d], tp=other).wait_recv()

    row_send(0, 0, 1, 0).start()
    row_send(0, 1, 2, 1).start()
    row_send(0, 1, 1, 2).start()
    row_send(0, 0, 2, 3).start()
    twin(0).start()

    ri = lax.broadcasted_iota(jnp.int32, (length, length), 0)
    ci = lax.broadcasted_iota(jnp.int32, (length, length), 1)
    tril = (ri >= ci).astype(F32)
    triu = (ri <= ci).astype(F32)
    high = lax.Precision.HIGHEST
    heads = leak.shape[2]
    lsum = jnp.dot(tril, leak[0], precision=high, preferred_element_type=F32)
    lsum_t = jnp.dot(leak_t[...], triu, precision=high, preferred_element_type=F32)
    for h in range(heads):
        lcol[h] = jnp.broadcast_to(lsum[:, h : h + 1], (length, wide))
        lrow[h] = jnp.broadcast_to(lsum_t[h : h + 1, :], (8, length))

    outs = (cow, how)

    def own_out(j, to_d, slot):
        return remote(outs[j], wo.at[f, j], os_.at[slot], or_.at[to_d, j], fs=f ^ to_d)

    def relay_out(d, j, to_d, slot):
        g = f ^ d
        return remote(wo.at[g, j], wo.at[g, j], os_.at[slot], or_.at[d ^ to_d, j], fs=f ^ to_d)

    def out_arrived(d, j):
        g = f ^ d
        remote(wo.at[g, j], wo.at[g, j], os_.at[0], or_.at[d, j], fs=f ^ 1).wait_recv()

    for j in range(2):
        pltpu.make_async_copy(outs[j], wo.at[f, j], oloc.at[j]).start()

    zrelay(0)
    row_arrived(1, 0)
    row_send(1, 0, 2, 4).start()
    row_arrived(2, 1)
    row_send(2, 1, 1, 5).start()
    own_out(0, 1, 0).start()
    own_out(1, 2, 1).start()
    zrelay(1)
    row_arrived(1, 1)
    twin(1).start()
    row_arrived(2, 0)
    twin(2).start()
    zrelay(2)
    row_arrived(3, 0)
    row_arrived(3, 1)
    twin(3).start()
    for d in range(nf):
        twin_arrived(d)

    def project(p):
        def one(g, carry):
            psend[g, p] = jnp.dot(rows[g], wg[p], preferred_element_type=F32).astype(BF)
            return carry

        lax.fori_loop(0, nf, one, 0)
        for d in range(1, nf):
            returned(d, p).start()
        prev[f, p] = psend[f, p]

    def returned(d, p):
        g = f ^ d
        return remote(psend.at[g, p], prev.at[f, p], ps.at[d, p], pr.at[d, p], fs=g)

    def returned_arrived(d, p):
        g = f ^ d
        remote(psend.at[g, p], prev.at[g, p], ps.at[d, p], pr.at[d, p], fs=g).wait_recv()

    def gathered(p):
        for d in range(1, nf):
            returned_arrived(d, p)

    project(0)
    project(1)
    project(2)
    own_out(1, 1, 2).start()
    own_out(0, 2, 3).start()
    zrelay(3)
    project(3)
    zrelay(4)
    project(4)
    out_arrived(1, 0)
    relay_out(1, 0, 2, 4).start()
    out_arrived(2, 1)
    relay_out(2, 1, 1, 5).start()

    for p in range(3):
        gathered(p)
    causal = ri >= ci
    tril_short = tril.astype(BF)

    def local(h, carry):
        fl = floor[h]
        logits = prev[h, FORGET].astype(F32)
        retain = fl + (1.0 - fl) * jax.nn.sigmoid(logits)
        keys = (1.0 - fl) * jax.nn.sigmoid(-logits)
        step = jnp.log(retain)
        coarse = step.astype(BF)
        fine = (step - coarse.astype(F32)).astype(BF)
        both = jnp.dot(
            tril_short, jnp.concatenate([coarse, fine], axis=1), preferred_element_type=F32
        )
        total = both[:, :wide] + both[:, wide:]
        raw = prev[h, QUERY].astype(F32)
        query = raw * jax.nn.sigmoid(raw) * jnp.exp(total)
        value = prev[h, VALUE]
        scores = lax.dot_general(
            query.astype(BF), (keys * jnp.exp(-total)).astype(BF), NT, preferred_element_type=F32
        )
        lc = lcol[h]
        gap = lc[:, 0:1] - lrow[h, 0:1, :]
        scores = jnp.where(causal, scores * jnp.exp(jnp.where(causal, gap, 0.0)), 0.0)
        inside[h] = jnp.dot(scores.astype(BF), value, preferred_element_type=F32)
        reach[h] = (query * jnp.exp(lc)).astype(BF)
        full = total + lc
        end = full[length - 1 :, :]
        update = (keys * jnp.exp(end - full)).astype(BF)
        states[h] = lax.dot_general(value, update, TN, preferred_element_type=F32)
        sdecay[h] = jnp.broadcast_to(jnp.exp(end), (8, wide))
        return carry

    lax.fori_loop(0, heads, local, 0)

    gathered(3)
    edge = rim.shape[1]

    def rim_copy(g):
        return remote(
            prev.at[g, SIGNAL, pl.ds(length - edge, edge), :], rim.at[g],
            ms.at[g], mr.at[g], sp=s + 1,
        )

    for g in range(nf):
        @pl.when(has_right)
        def _(g=g):
            rim_copy(g).start()

        @pl.when(s == 0)
        def _(g=g):
            rim[g] = jnp.zeros((edge, wide), BF)

    def state_copy(h):
        return remote(sout.at[h], sin.at[h], ss.at[h], sr.at[h], sp=s + 1)

    def chain(h, carry):
        @pl.when(has_left)
        def _():
            state_copy(h).wait_recv()

        @pl.when(s == 0)
        def _():
            sin[h] = jnp.zeros(sin.shape[1:], BF)

        @pl.when(has_right)
        def _():
            sout[h] = (sin[h].astype(F32) * sdecay[h, 0:1, :] + states[h]).astype(BF)
            state_copy(h).start()

        raw = inside[h] + lax.dot_general(reach[h], sin[h], NT, preferred_element_type=F32)
        scale = lax.rsqrt(jnp.mean(raw * raw, axis=-1, keepdims=True) + 1e-06)
        mix[1, :, pl.ds(pl.multiple_of(h * wide, wide), wide)] = (
            raw * scale * hgain[...]
        ).astype(BF)
        return carry

    lax.fori_loop(0, heads, chain, 0)
    gathered(4)

    for g in range(nf):
        @pl.when(has_left)
        def _(g=g):
            rim_copy(g).wait_recv()

    def conv(g, carry):
        padded = jnp.concatenate([rim[g], prev[g, SIGNAL]], axis=0).astype(F32)
        margin = taps.shape[1] - 1
        filtered = jnp.zeros((length, wide), F32)
        for o in range(margin + 1):
            start = edge - margin + o
            filtered = filtered + taps[g, o : o + 1, :] * padded[start : start + length]
        mix[0, :, pl.ds(pl.multiple_of(g * wide, wide), wide)] = (
            prev[g, GATE].astype(F32) * filtered
        ).astype(BF)
        return carry

    lax.fori_loop(0, nf, conv, 0)

    def partial(c, who):
        at = pl.ds(pl.multiple_of(who * half, half), half)
        return jnp.dot(mix[0, at, :], wo[c, 0], preferred_element_type=F32) + jnp.dot(
            mix[1, at, :], wo[c, 1], preferred_element_type=F32
        )

    def share(d):
        return remote(osend.at[d], orecv.at[d], es.at[d], er.at[d], tp=other)

    for j in range(2):
        pltpu.make_async_copy(outs[j], wo.at[f, j], oloc.at[j]).wait()
    cols = wo.shape[3]
    for d in range(nf):
        if d:
            for j in range(2):
                if (d, j) not in ((1, 0), (2, 1)):
                    out_arrived(d, j)
        c = f ^ d
        osend[d] = partial(c, other)
        share(d).start()
        at = pl.ds(pl.multiple_of(c * cols, cols), cols)
        mine = partial(c, t)
        share(d).wait_recv()
        out[0, :, at] = (mine + orecv[d]).astype(BF)

    for p in range(np_):
        def drained(b, carry, p=p):
            @pl.when(((b < s) & has_right) | ((b > s) & has_left))
            def _():
                relay(b, p, s).wait_send()

            return carry

        lax.fori_loop(0, ns, drained, 0)

        @pl.when(has_right)
        def _(p=p):
            own_right(p).wait_send()

        @pl.when(has_left)
        def _(p=p):
            own_left(p).wait_send()

        for d in range(1, nf):
            returned(d, p).wait_send()
    for d, j, to_d, slot in ((0, 0, 1, 0), (0, 1, 2, 1), (0, 1, 1, 2), (0, 0, 2, 3), (1, 0, 2, 4), (2, 1, 1, 5)):
        row_send(d, j, to_d, slot).wait_send()
        if d == 0:
            own_out(j, to_d, slot).wait_send()
        else:
            relay_out(d, j, to_d, slot).wait_send()
    for d in range(nf):
        twin(d).wait_send()
        share(d).wait_send()

    @pl.when(has_right)
    def _():
        for h in range(heads):
            state_copy(h).wait_send()
        for g in range(nf):
            rim_copy(g).wait_send()


def body(ns, nf, tokens, norm_gain, w0, w1, w2, w3, w4, conv_taps, floor_gate, leak, head_gain, cow, how):
    half, width = tokens.shape[1:]
    length = 2 * half
    heads = leak.shape[2]
    kd = w0.shape[0]
    wide = w0.shape[1] // nf
    assert heads == nf and nf == 4 and floor_gate.shape[0] == heads * wide
    taps = conv_taps.reshape(conv_taps.shape[0], nf, wide).transpose(1, 0, 2)
    vm = pl.BlockSpec(memory_space=pltpu.VMEM)
    dma = pltpu.SemaphoreType.DMA
    scratch = [
        pltpu.VMEM((nf, length, width), BF),
        pltpu.VMEM((5, ns * kd, wide), BF),
        pltpu.VMEM((nf, 5, length, wide), BF),
        pltpu.VMEM((nf, 5, length, wide), BF),
        pltpu.VMEM((nf, 2) + cow.shape, BF),
        pltpu.VMEM((nf, 16, wide), BF),
        pltpu.VMEM((heads, length, wide), F32),
        pltpu.VMEM((heads, length, wide), BF),
        pltpu.VMEM((heads, wide, wide), F32),
        pltpu.VMEM((heads, 8, wide), F32),
        pltpu.VMEM((heads, wide, wide), BF),
        pltpu.VMEM((heads, wide, wide), BF),
        pltpu.VMEM((heads, length, wide), F32),
        pltpu.VMEM((heads, 8, length), F32),
        pltpu.VMEM((2, length, heads * wide), BF),
        pltpu.VMEM((nf, half, cow.shape[1]), F32),
        pltpu.VMEM((nf, half, cow.shape[1]), F32),
        pltpu.VMEM((2, 5, half, wide), BF),
        dma((ns, 5)), dma((5,)), dma((ns, 5)), dma((5,)),
        dma((6,)), dma((nf, 2)), dma((nf,)), dma((nf,)),
        dma((nf, 5)), dma((nf, 5)),
        dma((6,)), dma((nf, 2)), dma((2,)),
        dma((nf,)), dma((nf,)), dma((heads,)), dma((heads,)),
        dma((nf,)), dma((nf,)),
        dma((2, 5)), dma((2, 5)), dma((2, 5)), dma((2, 5)),
    ]
    return pl.pallas_call(
        functools.partial(kernel, ns, nf),
        out_shape=jax.ShapeDtypeStruct(tokens.shape, BF),
        in_specs=[vm] * 14,
        out_specs=vm,
        scratch_shapes=scratch,
        compiler_params=pltpu.CompilerParams(
            collective_id=0, has_side_effects=True, vmem_limit_bytes=60 * 2**20
        ),
    )(
        tokens, norm_gain[None], w0, w1, w2, w3, w4, taps, floor_gate.reshape(heads, 1, wide),
        leak, leak[0].T, head_gain[None], cow, how,
    )


def solution(mesh):
    in_specs = (
        P("fs", ("sp", "tp"), None),
        P(),
        P("sp", "tp"),
        P("sp", "tp"),
        P("sp", "tp"),
        P("sp", "tp"),
        P("sp", "tp"),
        P(None, "tp"),
        P("tp"),
        P("fs", "sp", "tp"),
        P(),
        P("tp", "fs"),
        P("tp", "fs"),
    )
    out_specs = P("fs", ("sp", "tp"), None)
    step = functools.partial(body, mesh.shape["sp"], mesh.shape["fs"])
    return jax.shard_map(step, mesh=mesh, in_specs=in_specs, out_specs=out_specs, check_vma=False)
```

profile of v0, /device:TPU:9, one launch (start us, length us, event | category | flops | bytes accessed | tf_op | source)
XLA Modules:
  0.0 95.2 jit_solution(16257246778117559449)
XLA Ops:
  0.0 0.0 copy-start
  0.0 0.7 copy-done
  0.7 0.8 copy.14.leak
  1.5 91.6 %shard_map.127 = bf16[1,192,2048]{2,1,0:T(8,128)(2,1)} custom-call(bf16[1,192,2048]{2,1,0:T(8,128)(2,1)} %tok.1, f32[1,2048]{1,0:T(1,128)} %bitcast.10, bf16[512,512]{1,0:T(8,128)(2,1)} %w0.1, bf16[512,512]{1,0:T(8,128)(2,1)} %w1.1, bf16[512,512]{1,0:T(8,128)(2,1)} %w2.1, bf16[512,512]{1,0:T(8,128)(2,1)} %w3.1, bf16[512,512]{1,0:T(8,128)(2,1)} %w4.1, ...), custom_call_target="tpu_custom_call" | custom-call | tf_op jit(solution)/shard_map/pallas_call | solution.py:434
  93.1 2.1 %copy.16 = bf16[1,192,2048]{2,1,0:T(8,128)(2,1)} copy(bf16[1,192,2048]{2,1,0:T(8,128)(2,1)} %shard_map.127) | data formatting | bytes 1572864
Async XLA Ops:
  0.0 0.7 copy-start
where the time goes:
time: 96 us; the launch traced here: 95.2 us
  Pallas kernels  91.6 us (95%)
  local copies, waits for them, and re-layouts  3.6 us (4%)
    pallas_call x1, Pallas kernels, body(): pl.pallas_call(functools.partial(kernel, ns, nf), out_shape=jax.ShapeDtyp...  91.6 us
    unnamed x4, local copies, waits for them, and re-layouts  3.6 us

commit v1 on v0

v1 whole, which is shorter than its diff:
```python
import functools

import jax
import jax.numpy as jnp
from jax import lax
from jax.experimental import pallas as pl
from jax.experimental.pallas import tpu as pltpu
from jax.sharding import PartitionSpec as P

MESH = pl.DeviceIdType.MESH
BF = jnp.bfloat16
F32 = jnp.float32
NT = (((1,), (1,)), ((), ()))
TN = (((0,), (0,)), ((), ()))
GATE, SIGNAL, QUERY, FORGET, VALUE = 4, 3, 1, 0, 2


def kernel(
    ns, nf,
    tok, gain, w0, w1, w2, w3, w4, taps, floor, leak_t, hgain, cow, how,
    out,
    tokv, rows, wg, y, wo, rim, inside, reach, states, sdecay, sin, sout,
    lk, lcol, lrow, msend, mix, osend, orecv, mine,
    tl, zs, zsl, zr, zloc, rs, rr, ts, tr, ls, lr, oloc, os_, or_, rl, za, xs, xr, ms, mr, ss, sr, es, er,
):
    s, f, t = lax.axis_index("sp"), lax.axis_index("fs"), lax.axis_index("tp")
    other = 1 - t
    half = tok.shape[1]
    length = 2 * half
    kd = w0.shape[0]
    wide = w0.shape[1] // nf
    ws = (w3, w2, w4, w1, w0)
    np_ = len(ws)
    has_left, has_right = s > 0, s < ns - 1
    outs = (cow, how)
    cols = wo.shape[3]
    odd = lax.rem(s, 2)
    mate = s + 1 - 2 * odd

    def remote(src, dst, send, recv, **where):
        return pltpu.make_async_remote_copy(
            src_ref=src, dst_ref=dst, send_sem=send, recv_sem=recv,
            device_id=where, device_id_type=MESH,
        )

    def wblock(b, p):
        return wg.at[p, pl.ds(pl.multiple_of(b * kd, kd), kd), :]

    def wload(p):
        return pltpu.make_async_copy(
            ws[p].at[:, pl.ds(pl.multiple_of(f * wide, wide), wide)], wblock(s, p), zloc.at[p]
        )

    def oload(j):
        return pltpu.make_async_copy(outs[j], wo.at[f, j], oloc.at[j])

    tload = pltpu.make_async_copy(tok.at[0], tokv, tl.at[0])
    wload(0).start()
    tload.start()
    for p in range(1, np_):
        wload(p).start()
    for j in range(2):
        oload(j).start()

    barrier = pltpu.get_barrier_semaphore()
    pl.semaphore_signal(barrier, inc=1, device_id={"tp": other}, device_id_type=MESH)
    for d in range(1, nf):
        pl.semaphore_signal(barrier, inc=1, device_id={"fs": f ^ d}, device_id_type=MESH)

    @pl.when(has_left)
    def _():
        pl.semaphore_signal(barrier, inc=1, device_id={"sp": s - 1}, device_id_type=MESH)

    @pl.when(has_right)
    def _():
        pl.semaphore_signal(barrier, inc=1, device_id={"sp": s + 1}, device_id_type=MESH)

    heads = leak_t.shape[0]
    lk[f, pl.ds(0, heads), :] = leak_t[...]
    ends = jnp.where(has_left, 1, 0) + jnp.where(has_right, 1, 0)
    pl.semaphore_wait(barrier, nf + ends)


    def own_right(p):
        return remote(wblock(s, p), wblock(s, p), zs.at[s, p], zr.at[s, p], sp=s + 1)

    def own_left(p):
        return remote(wblock(s, p), wblock(s, p), zsl.at[p], zr.at[s, p], sp=s - 1)

    def relay(b, p, to):
        return remote(wblock(b, p), wblock(b, p), zs.at[b, p], zr.at[b, p], sp=to)

    def send_own(p):
        wload(p).wait()

        @pl.when(has_right)
        def _():
            own_right(p).start()

        @pl.when(has_left)
        def _():
            own_left(p).start()

    def zhop(k, p):
        @pl.when((s - k >= 0) & has_right)
        def _():
            relay(s - k, p, s + 1).wait_recv()
            relay(s - k, p, s + 1).start()

        @pl.when((s + k < ns) & has_left)
        def _():
            relay(s + k, p, s - 1).wait_recv()
            relay(s + k, p, s - 1).start()

    def zfar(p):
        def hop(k, carry):
            zhop(k, p)
            return carry

        if ns > 3:
            lax.fori_loop(3, ns, hop, 0)

    def zready(p):
        def hop(k, carry):
            @pl.when((s - k >= 0) & (s == ns - 1))
            def _():
                relay(s - k, p, s - 1).wait_recv()

            @pl.when((s + k < ns) & (s == 0))
            def _():
                relay(s + k, p, s + 1).wait_recv()

            return carry

        lax.fori_loop(1, ns, hop, 0)

    send_own(0)
    send_own(1)


    tload.wait()
    x = tokv[...].astype(F32)
    center = x - jnp.mean(x, axis=-1, keepdims=True)
    spread = jnp.mean(center * center, axis=-1, keepdims=True)
    rows[f, pl.ds(pl.multiple_of(t * half, half), half), :] = (
        center * lax.rsqrt(spread + 1e-05) * gain[...]
    ).astype(BF)

    quarter = half // 2

    def piece(g, j):
        return rows.at[g, pl.ds(pl.multiple_of(t * half + j * quarter, quarter), quarter), :]

    def core_rows(g, core):
        return rows.at[g, pl.ds(pl.multiple_of(core * half, half), half), :]

    def row_arrived(d, j):
        g = f ^ d
        remote(piece(g, j), piece(g, j), rs.at[0], rr.at[d, j], fs=f ^ 1).wait_recv()

    def row_send(d, j, to_d, slot):
        g = f ^ d
        to = f ^ to_d
        return remote(piece(g, j), piece(g, j), rs.at[slot], rr.at[d ^ to_d, j], fs=to)

    def twin(d):
        g = f ^ d
        return remote(core_rows(g, t), core_rows(g, t), ts.at[d], tr.at[d], tp=other)

    def twin_arrived(d):
        g = f ^ d
        remote(core_rows(g, other), core_rows(g, other), ts.at[d], tr.at[d], tp=other).wait_recv()

    def leak_send(d):
        return remote(lk.at[f], lk.at[f], ls.at[d], lr.at[d], fs=f ^ d)

    def leak_arrived(d):
        g = f ^ d
        remote(lk.at[g], lk.at[g], ls.at[d], lr.at[d], fs=g).wait_recv()

    for d in range(1, nf):
        leak_send(d).start()
    row_send(0, 0, 1, 0).start()
    row_send(0, 1, 2, 1).start()
    row_send(0, 1, 1, 2).start()
    row_send(0, 0, 2, 3).start()
    twin(0).start()

    zhop(1, 0)
    zhop(1, 1)
    zhop(2, 0)
    send_own(2)


    for d in range(1, nf):
        leak_arrived(d)
    ri = lax.broadcasted_iota(jnp.int32, (length, length), 0)
    ci = lax.broadcasted_iota(jnp.int32, (length, length), 1)
    tril = (ri >= ci).astype(F32)
    triu = (ri <= ci).astype(F32)
    high = lax.Precision.HIGHEST
    mine_leak = jnp.concatenate(
        [lk[g, pl.ds(f, 1), :] for g in range(nf)] + [jnp.zeros((8 - nf, length), F32)], axis=0
    )
    lsum = lax.dot_general(tril, mine_leak, NT, precision=high, preferred_element_type=F32)
    lsum_t = jnp.dot(mine_leak, triu, precision=high, preferred_element_type=F32)
    for g in range(nf):
        lcol[g] = jnp.broadcast_to(lsum[:, g : g + 1], (length, wide))
        lrow[g] = jnp.broadcast_to(lsum_t[g : g + 1, :], (8, length))


    pw = cols // 4

    def opiece(g, q):
        return wo.at[g, :, :, pl.ds(pl.multiple_of(q * pw, pw), pw)]

    def order(to_d, i):
        first = 2 * odd + (1 if to_d == 1 else 0)
        second = 2 * odd + (0 if to_d == 1 else 1)
        return (first, second, 2 - 2 * odd, 3 - 2 * odd)[i]

    def own_out(to_d, i):
        q = order(to_d, i)
        return remote(opiece(f, q), opiece(f, q), os_.at[to_d, i], or_.at[to_d, q], fs=f ^ to_d)

    def out_arrived(d, q):
        g = f ^ d
        remote(opiece(g, q), opiece(g, q), os_.at[1, 0], or_.at[d, q], fs=f ^ 1).wait_recv()

    def relay_out(d, to_d):
        g = f ^ d
        q = order(d, 0)
        return remote(opiece(g, q), opiece(g, q), rl.at[to_d], or_.at[3, q], fs=f ^ to_d)

    def assist(i):
        g = f ^ 3
        q = 2 * odd + i
        return remote(opiece(g, q), opiece(g, q), za.at[i], or_.at[3, q], sp=mate)

    row_arrived(1, 0)
    row_send(1, 0, 2, 4).start()
    row_arrived(2, 1)
    row_send(2, 1, 1, 5).start()
    for j in range(2):
        oload(j).wait()
    for i in range(2):
        own_out(1, i).start()
        own_out(2, i).start()

    zhop(1, 2)
    zhop(2, 1)
    zfar(0)
    zready(0)

    def project(d, p):
        g = f ^ d
        y[g, p] = jnp.dot(rows[g], wg[p], preferred_element_type=F32).astype(BF)

    twin_arrived(0)
    project(0, 0)
    zhop(2, 2)
    send_own(3)
    row_arrived(1, 1)
    twin(1).start()
    row_arrived(2, 0)
    twin(2).start()
    zhop(1, 3)
    send_own(4)
    zfar(1)
    zready(1)
    project(0, 1)
    zhop(1, 4)
    zfar(2)
    zready(2)
    project(0, 2)
    zhop(2, 3)

    causal = ri >= ci
    tril_short = tril.astype(BF)

    def local(d):
        g = f ^ d
        fl = floor[f]
        logits = y[g, FORGET].astype(F32)
        retain = fl + (1.0 - fl) * jax.nn.sigmoid(logits)
        keys = (1.0 - fl) * jax.nn.sigmoid(-logits)
        step = jnp.log(retain)
        coarse = step.astype(BF)
        fine = (step - coarse.astype(F32)).astype(BF)
        both = jnp.dot(
            tril_short, jnp.concatenate([coarse, fine], axis=1), preferred_element_type=F32
        )
        total = both[:, :wide] + both[:, wide:]
        raw = y[g, QUERY].astype(F32)
        query = raw * jax.nn.sigmoid(raw) * jnp.exp(total)
        value = y[g, VALUE]
        scores = lax.dot_general(
            query.astype(BF), (keys * jnp.exp(-total)).astype(BF), NT, preferred_element_type=F32
        )
        lc = lcol[g]
        gap = lc[:, 0:1] - lrow[g, 0:1, :]
        scores = jnp.where(causal, scores * jnp.exp(jnp.where(causal, gap, 0.0)), 0.0)
        inside[g] = jnp.dot(scores.astype(BF), value, preferred_element_type=F32)
        reach[g] = (query * jnp.exp(lc)).astype(BF)
        full = total + lc
        end = full[length - 1 :, :]
        update = (keys * jnp.exp(end - full)).astype(BF)
        states[g] = lax.dot_general(value, update, TN, preferred_element_type=F32)
        sdecay[g] = jnp.broadcast_to(jnp.exp(end), (8, wide))

    def many(body, first, last):
        def one(d, carry):
            body(d)
            return carry

        lax.fori_loop(first, last, one, 0)

    def project_chain(d):
        for p in range(3):
            project(d, p)

    row_arrived(3, 0)
    row_arrived(3, 1)
    twin(3).start()
    local(0)
    zhop(2, 4)
    twin_arrived(1)
    twin_arrived(2)

    def both_steps(d):
        project_chain(d)
        local(d)

    many(both_steps, 1, 3)
    twin_arrived(3)
    many(both_steps, 3, 4)

    out_arrived(2, order(2, 0))
    relay_out(2, 1).start()
    out_arrived(1, order(1, 0))
    relay_out(1, 2).start()
    own_out(1, 2).start()
    own_out(2, 2).start()

    def state_copy(g):
        return remote(sout.at[g], sin.at[g], ss.at[g], sr.at[g], sp=s + 1)

    def place(j, g):
        return mix.at[j, :, pl.ds(pl.multiple_of(g * wide, wide), wide)]

    def mixed_send(d, j):
        return remote(msend.at[d, j], place(j, f), xs.at[d, j], xr.at[d, j], fs=f ^ d)

    def mixed_arrived(d, j):
        remote(msend.at[d, j], place(j, f ^ d), xs.at[d, j], xr.at[d, j], fs=f ^ d).wait_recv()

    def deliver(d, j, value):
        @pl.when(d == 0)
        def _():
            mix[j, :, pl.ds(pl.multiple_of(f * wide, wide), wide)] = value

        @pl.when(d > 0)
        def _():
            msend[d, j] = value
            mixed_send(d, j).start()

    def chain(d):
        g = f ^ d

        @pl.when(has_left)
        def _():
            state_copy(g).wait_recv()

        @pl.when(s == 0)
        def _():
            sin[g] = jnp.zeros(sin.shape[1:], BF)

        @pl.when(has_right)
        def _():
            sout[g] = (sin[g].astype(F32) * sdecay[g, 0:1, :] + states[g]).astype(BF)
            state_copy(g).start()

        raw = inside[g] + lax.dot_general(reach[g], sin[g], NT, preferred_element_type=F32)
        scale = lax.rsqrt(jnp.mean(raw * raw, axis=-1, keepdims=True) + 1e-06)
        deliver(d, 1, (raw * scale * hgain[...]).astype(BF))

    many(chain, 0, nf)


    edge = rim.shape[1]

    def rim_copy(g):
        return remote(
            y.at[g, SIGNAL, pl.ds(length - edge, edge), :], rim.at[g],
            ms.at[g], mr.at[g], sp=s + 1,
        )

    zfar(3)
    zready(3)

    def signal(d):
        g = f ^ d
        project(d, 3)

        @pl.when(has_right)
        def _():
            rim_copy(g).start()

        @pl.when(s == 0)
        def _():
            rim[g] = jnp.zeros((edge, wide), BF)

    many(signal, 0, nf)
    zfar(4)
    zready(4)

    def conv(d):
        g = f ^ d
        project(d, 4)

        @pl.when(has_left)
        def _():
            rim_copy(g).wait_recv()

        padded = jnp.concatenate([rim[g], y[g, SIGNAL]], axis=0).astype(F32)
        margin = taps.shape[1] - 1
        filtered = jnp.zeros((length, wide), F32)
        for o in range(margin + 1):
            start = edge - margin + o
            filtered = filtered + taps[f, o : o + 1, :] * padded[start : start + length]
        deliver(d, 0, (y[g, GATE].astype(F32) * filtered).astype(BF))

    many(conv, 0, nf)
    own_out(1, 3).start()
    own_out(2, 3).start()
    for i in range(2):
        out_arrived(3, 2 * odd + i)
        assist(i).start()


    def share(i):
        return remote(osend.at[i], orecv.at[i], es.at[i], er.at[i], tp=other)

    for d in range(1, nf):
        for j in range(2):
            mixed_arrived(d, j)

    def partial(g, c, who):
        at = pl.ds(pl.multiple_of(who * half, half), half)
        co = pl.ds(pl.multiple_of(c * 2 * pw, 2 * pw), 2 * pw)
        return jnp.dot(mix[0, at, :], wo[g, 0, :, co], preferred_element_type=F32) + jnp.dot(
            mix[1, at, :], wo[g, 1, :, co], preferred_element_type=F32
        )

    def begin(i, d, c):
        g = f ^ d
        osend[i] = partial(g, c, other)
        share(i).start()
        mine[i] = partial(g, c, t)

    def finish(i, d, c):
        g = f ^ d
        share(i).wait_recv()
        at = pl.ds(pl.multiple_of(g * cols + c * 2 * pw, 2 * pw), 2 * pw)
        out[0, :, at] = (mine[i] + orecv[i]).astype(BF)

    plan = [
        (0, odd, ()),
        (0, 1 - odd, ()),
        (1, odd, (order(1, 1),)),
        (2, odd, (order(2, 1),)),
        (3, odd, ()),
        (3, 1 - odd, (2 - 2 * odd, 3 - 2 * odd)),
        (1, 1 - odd, (2 - 2 * odd, 3 - 2 * odd)),
        (2, 1 - odd, (2 - 2 * odd, 3 - 2 * odd)),
    ]
    for i, (d, c, waits) in enumerate(plan):
        for q in waits:
            out_arrived(d, q)
        begin(i, d, c)
        if i:
            finish(i - 1, *plan[i - 1][:2])
    finish(len(plan) - 1, *plan[-1][:2])


    for p in range(np_):
        def drained(b, carry, p=p):
            @pl.when(((b < s) & has_right) | ((b > s) & has_left))
            def _():
                relay(b, p, s).wait_send()

            return carry

        lax.fori_loop(0, ns, drained, 0)

        @pl.when(has_right)
        def _(p=p):
            own_right(p).wait_send()

        @pl.when(has_left)
        def _(p=p):
            own_left(p).wait_send()

    for d, j, to_d, slot in ((0, 0, 1, 0), (0, 1, 2, 1), (0, 1, 1, 2), (0, 0, 2, 3), (1, 0, 2, 4), (2, 1, 1, 5)):
        row_send(d, j, to_d, slot).wait_send()
    for to_d in range(1, 3):
        for i in range(4):
            own_out(to_d, i).wait_send()
        relay_out(3 - to_d, to_d).wait_send()
    for i in range(2):
        assist(i).wait_send()
    for d in range(nf):
        twin(d).wait_send()
        if d:
            leak_send(d).wait_send()
            for j in range(2):
                mixed_send(d, j).wait_send()
    for i in range(len(plan)):
        share(i).wait_send()

    @pl.when(has_right)
    def _():
        for g in range(nf):
            state_copy(g).wait_send()
            rim_copy(g).wait_send()


def body(ns, nf, tokens, norm_gain, w0, w1, w2, w3, w4, conv_taps, floor_gate, leak, head_gain, cow, how):
    half, width = tokens.shape[1:]
    length = 2 * half
    heads = leak.shape[2]
    kd = w0.shape[0]
    wide = w0.shape[1] // nf
    assert heads == nf and nf == 4 and floor_gate.shape[0] == heads * wide and ns % 2 == 0
    taps = conv_taps.reshape(conv_taps.shape[0], nf, wide).transpose(1, 0, 2)
    vm = pl.BlockSpec(memory_space=pltpu.VMEM)
    hbm = pl.BlockSpec(memory_space=pl.ANY)
    dma = pltpu.SemaphoreType.DMA
    cols = cow.shape[1]
    scratch = [
        pltpu.VMEM((half, width), BF),
        pltpu.VMEM((nf, length, width), BF),
        pltpu.VMEM((5, ns * kd, wide), BF),
        pltpu.VMEM((nf, 5, length, wide), BF),
        pltpu.VMEM((nf, 2) + cow.shape, BF),
        pltpu.VMEM((nf, 16, wide), BF),
        pltpu.VMEM((nf, length, wide), F32),
        pltpu.VMEM((nf, length, wide), BF),
        pltpu.VMEM((nf, wide, wide), F32),
        pltpu.VMEM((nf, 8, wide), F32),
        pltpu.VMEM((nf, wide, wide), BF),
        pltpu.VMEM((nf, wide, wide), BF),
        pltpu.VMEM((nf, 8, length), F32),
        pltpu.VMEM((nf, length, wide), F32),
        pltpu.VMEM((nf, 8, length), F32),
        pltpu.VMEM((nf, 2, length, wide), BF),
        pltpu.VMEM((2, length, nf * wide), BF),
        pltpu.VMEM((2 * nf, half, cols // 2), F32),
        pltpu.VMEM((2 * nf, half, cols // 2), F32),
        pltpu.VMEM((2 * nf, half, cols // 2), F32),
        dma((1,)), dma((ns, 5)), dma((5,)), dma((ns, 5)), dma((5,)),
        dma((6,)), dma((nf, 2)), dma((nf,)), dma((nf,)), dma((nf,)), dma((nf,)),
        dma((2,)), dma((3, 4)), dma((nf, 4)), dma((3,)), dma((2,)),
        dma((nf, 2)), dma((nf, 2)), dma((nf,)), dma((nf,)), dma((nf,)), dma((nf,)),
        dma((2 * nf,)), dma((2 * nf,)),
    ]
    return pl.pallas_call(
        functools.partial(kernel, ns, nf),
        out_shape=jax.ShapeDtypeStruct(tokens.shape, BF),
        in_specs=[hbm, vm, hbm, hbm, hbm, hbm, hbm, vm, vm, vm, vm, hbm, hbm],
        out_specs=vm,
        scratch_shapes=scratch,
        compiler_params=pltpu.CompilerParams(
            collective_id=0, has_side_effects=True, vmem_limit_bytes=48 * 2**20
        ),
    )(
        tokens, norm_gain[None], w0, w1, w2, w3, w4, taps, floor_gate.reshape(heads, 1, wide),
        leak[0].T, head_gain[None], cow, how,
    )


def solution(mesh):
    in_specs = (
        P("fs", ("sp", "tp"), None),
        P(),
        P("sp", "tp"),
        P("sp", "tp"),
        P("sp", "tp"),
        P("sp", "tp"),
        P("sp", "tp"),
        P(None, "tp"),
        P("tp"),
        P("fs", "sp", "tp"),
        P(),
        P("tp", "fs"),
        P("tp", "fs"),
    )
    out_specs = P("fs", ("sp", "tp"), None)
    step = functools.partial(body, mesh.shape["sp"], mesh.shape["fs"])
    return jax.shard_map(step, mesh=mesh, in_specs=in_specs, out_specs=out_specs, check_vma=False)
```

time: 96 us -> 87.1 us (0.907)
  Pallas kernels: 91.6 us -> 74.4 us
  local copies, waits for them, and re-layouts: 3.6 us -> 12.1 us
    pallas_call x1, Pallas kernels: 91.6 us -> 74.4 us  [body(): pl.pallas_call(functools.partial(kernel, ns, nf), out_shape=jax.ShapeDtyp...]
    unnamed x4 -> x27, local copies, waits for them, and re-layouts: 3.6 us -> 12.1 us
where the time goes in v1:
time: 87.1 us; the launch traced here: 86.5 us
  Pallas kernels  74.4 us (85%)
  local copies, waits for them, and re-layouts  12.1 us (14%)
    pallas_call x1, Pallas kernels, body(): pl.pallas_call(functools.partial(kernel, ns, nf), out_shape=jax.ShapeDtyp...  74.4 us
    unnamed x27, local copies, waits for them, and re-layouts  12.1 us

profile of v1, /device:TPU:9, one launch (start us, length us, event | category | flops | bytes accessed | tf_op | source)
XLA Modules:
  0.0 86.5 jit_solution(7078901535889519460)
XLA Ops:
  0.0 0.0 copy-start.8
  0.0 0.0 copy-start.12
  0.0 0.7 copy-done.8
  0.7 0.0 copy-done.12
  0.7 0.0 copy-start
  0.7 1.1 %copy-done = bf16[1,192,2048]{2,1,0:T(8,128)(2,1)S(1)} copy-done((bf16[1,192,2048]{2,1,0:T(8,128)(2,1)S(1)}, bf16[1,192,2048]{2,1,0:T(8,128)(2,1)}, u32[]{:S(2)}) %copy-start) | copy-done | bytes 786456
  1.8 0.0 copy-start.1
  1.8 1.0 %copy-done.1 = bf16[512,512]{1,0:T(8,128)(2,1)S(1)} copy-done((bf16[512,512]{1,0:T(8,128)(2,1)S(1)}, bf16[512,512]{1,0:T(8,128)(2,1)}, u32[]{:S(2)}) %copy-start.1) | copy-done | bytes 524312
  2.9 1.0 %copy-done.2 = bf16[512,512]{1,0:T(8,128)(2,1)S(1)} copy-done((bf16[512,512]{1,0:T(8,128)(2,1)S(1)}, bf16[512,512]{1,0:T(8,128)(2,1)}, u32[]{:S(2)}) %copy-start.2) | copy-done | bytes 524312
  3.9 0.0 copy-start.3
  3.9 1.0 %copy-done.3 = bf16[512,512]{1,0:T(8,128)(2,1)S(1)} copy-done((bf16[512,512]{1,0:T(8,128)(2,1)S(1)}, bf16[512,512]{1,0:T(8,128)(2,1)}, u32[]{:S(2)}) %copy-start.3) | copy-done | bytes 524312
  5.0 0.0 copy-start.4
  5.0 1.0 %copy-done.4 = bf16[512,512]{1,0:T(8,128)(2,1)S(1)} copy-done((bf16[512,512]{1,0:T(8,128)(2,1)S(1)}, bf16[512,512]{1,0:T(8,128)(2,1)}, u32[]{:S(2)}) %copy-start.4) | copy-done | bytes 524312
  6.0 0.0 copy-start.5
  6.0 1.0 %copy-done.5 = bf16[512,512]{1,0:T(8,128)(2,1)S(1)} copy-done((bf16[512,512]{1,0:T(8,128)(2,1)S(1)}, bf16[512,512]{1,0:T(8,128)(2,1)}, u32[]{:S(2)}) %copy-start.5) | copy-done | bytes 524312
  7.0 0.0 copy-start.6
  7.0 1.0 %copy-done.6 = bf16[512,512]{1,0:T(8,128)(2,1)S(1)} copy-done((bf16[512,512]{1,0:T(8,128)(2,1)S(1)}, bf16[512,512]{1,0:T(8,128)(2,1)}, u32[]{:S(2)}) %copy-start.6) | copy-done | bytes 524312
  8.1 0.0 copy-start.7
  8.1 1.0 %copy-done.7 = bf16[512,512]{1,0:T(8,128)(2,1)S(1)} copy-done((bf16[512,512]{1,0:T(8,128)(2,1)S(1)}, bf16[512,512]{1,0:T(8,128)(2,1)}, u32[]{:S(2)}) %copy-start.7) | copy-done | bytes 524312
  9.1 0.7 copy-done.9
  9.8 0.7 copy-done.10
  10.5 0.7 copy-done.11
  11.2 74.4 %shard_map.127 = bf16[1,192,2048]{2,1,0:T(8,128)(2,1)S(1)} custom-call(bf16[1,192,2048]{2,1,0:T(8,128)(2,1)S(1)} %copy-done, f32[1,2048]{1,0:T(1,128)S(1)} %bitcast.9, bf16[512,512]{1,0:T(8,128)(2,1)S(1)} %copy-done.1, bf16[512,512]{1,0:T(8,128)(2,1)S(1)} %copy-done.2, bf16[512,512]{1,0:T(8,128)(2,1)S(1)} %copy-done.3, bf16[512,512]{1,0:T(8,128)(2,1)S(1)} %copy-done.4, ...), custom_call_target="tpu_custom_call" | custom-call | tf_op jit(solution)/shard_map/pallas_call | solution.py:567
  85.6 0.9 %copy.15 = bf16[1,192,2048]{2,1,0:T(8,128)(2,1)} copy(bf16[1,192,2048]{2,1,0:T(8,128)(2,1)S(1)} %shard_map.127) | data formatting | bytes 1572864
  (4 shorter events, 0.0 us)
Async XLA Ops:
  0.0 0.7 copy-start.8
  0.0 0.7 copy-start.12
  0.7 1.1 %copy-start = (bf16[1,192,2048]{2,1,0:T(8,128)(2,1)S(1)}, bf16[1,192,2048]{2,1,0:T(8,128)(2,1)}, u32[]{:S(2)}) copy-start(bf16[1,192,2048]{2,1,0:T(8,128)(2,1)} %tok.1) | copy-start | bytes 2359300
  1.8 1.0 %copy-start.1 = (bf16[512,512]{1,0:T(8,128)(2,1)S(1)}, bf16[512,512]{1,0:T(8,128)(2,1)}, u32[]{:S(2)}) copy-start(bf16[512,512]{1,0:T(8,128)(2,1)} %w0.1) | copy-start | bytes 1572868
  2.9 1.0 %copy-start.2 = (bf16[512,512]{1,0:T(8,128)(2,1)S(1)}, bf16[512,512]{1,0:T(8,128)(2,1)}, u32[]{:S(2)}) copy-start(bf16[512,512]{1,0:T(8,128)(2,1)} %w1.1) | copy-start | bytes 1572868
  3.9 1.0 %copy-start.3 = (bf16[512,512]{1,0:T(8,128)(2,1)S(1)}, bf16[512,512]{1,0:T(8,128)(2,1)}, u32[]{:S(2)}) copy-start(bf16[512,512]{1,0:T(8,128)(2,1)} %w2.1) | copy-start | bytes 1572868
  5.0 1.0 %copy-start.4 = (bf16[512,512]{1,0:T(8,128)(2,1)S(1)}, bf16[512,512]{1,0:T(8,128)(2,1)}, u32[]{:S(2)}) copy-start(bf16[512,512]{1,0:T(8,128)(2,1)} %w3.1) | copy-start | bytes 1572868
  6.0 1.0 %copy-start.5 = (bf16[512,512]{1,0:T(8,128)(2,1)S(1)}, bf16[512,512]{1,0:T(8,128)(2,1)}, u32[]{:S(2)}) copy-start(bf16[512,512]{1,0:T(8,128)(2,1)} %w4.1) | copy-start | bytes 1572868
  7.0 1.0 %copy-start.6 = (bf16[512,512]{1,0:T(8,128)(2,1)S(1)}, bf16[512,512]{1,0:T(8,128)(2,1)}, u32[]{:S(2)}) copy-start(bf16[512,512]{1,0:T(8,128)(2,1)} %cow.1) | copy-start | bytes 1572868
  8.1 1.0 %copy-start.7 = (bf16[512,512]{1,0:T(8,128)(2,1)S(1)}, bf16[512,512]{1,0:T(8,128)(2,1)}, u32[]{:S(2)}) copy-start(bf16[512,512]{1,0:T(8,128)(2,1)} %how.1) | copy-start | bytes 1572868
  9.1 0.7 copy-start.9
  9.8 0.7 copy-start.10
  10.5 0.7 copy-start.11

commit v2 on v1

v2 whole, which is shorter than its diff:
```python
import functools

import jax
import jax.numpy as jnp
from jax import lax
from jax.experimental import pallas as pl
from jax.experimental.pallas import tpu as pltpu
from jax.sharding import PartitionSpec as P

MESH = pl.DeviceIdType.MESH
BF = jnp.bfloat16
F32 = jnp.float32
NT = (((1,), (1,)), ((), ()))
TN = (((0,), (0,)), ((), ()))
GATE, SIGNAL, QUERY, FORGET, VALUE = 4, 3, 1, 0, 2


def kernel(
    ns, nf,
    tok_h, gain_h, w0, w1, w2, w3, w4, taps_h, floor_h, leak_h, hgain_h, cow, how,
    out,
    tokv, gain, taps, floor, leak_t, hgain,
    rows, wg, y, wo, rim, filt, inside, reach, states, sdecay, sin, sout,
    lk, lcol, lrow, msend, mix, acc, orecv,
    il, zs, zsl, zr, zloc, rs, rr, ts, tr, ls, lr, oloc, os_, or_, rl, za, xs, xr, ms, mr, ss, sr, es, er,
):
    s, f, t = lax.axis_index("sp"), lax.axis_index("fs"), lax.axis_index("tp")
    other = 1 - t
    half = tokv.shape[0]
    length = 2 * half
    kd = w0.shape[0]
    wide = w0.shape[1] // nf
    ws = (w3, w2, w4, w1, w0)
    np_ = len(ws)
    has_left, has_right = s > 0, s < ns - 1
    inner = has_left & has_right
    outs = (cow, how)
    depth, cols = cow.shape
    odd = lax.rem(s, 2)
    mate = s + 1 - 2 * odd

    def remote(src, dst, send, recv, **where):
        return pltpu.make_async_remote_copy(
            src_ref=src, dst_ref=dst, send_sem=send, recv_sem=recv,
            device_id=where, device_id_type=MESH,
        )


    def wblock(b, p):
        return wg.at[pl.ds(pl.multiple_of(b * kd, kd), kd), pl.ds(p * wide, wide)]

    def wload(p):
        return pltpu.make_async_copy(
            ws[p].at[:, pl.ds(pl.multiple_of(f * wide, wide), wide)], wblock(s, p), zloc.at[p]
        )

    def oload(j):
        return pltpu.make_async_copy(outs[j], wo.at[0, pl.ds(j * depth, depth), :], oloc.at[j])

    loads = [
        pltpu.make_async_copy(src, dst, il.at[i])
        for i, (src, dst) in enumerate(
            ((tok_h.at[0], tokv), (gain_h, gain), (leak_h, leak_t), (taps_h, taps), (floor_h, floor), (hgain_h, hgain))
        )
    ]

    wload(0).start()
    loads[0].start()
    wload(1).start()
    for load in loads[1:]:
        load.start()
    for p in range(2, np_):
        wload(p).start()
    for j in range(2):
        oload(j).start()

    barrier = pltpu.get_barrier_semaphore()
    for d in range(nf - 1, 0, -1):
        pl.semaphore_signal(barrier, inc=1, device_id={"fs": f ^ d}, device_id_type=MESH)

    @pl.when(has_left)
    def _():
        pl.semaphore_signal(barrier, inc=1, device_id={"sp": s - 1}, device_id_type=MESH)

    @pl.when(has_right)
    def _():
        pl.semaphore_signal(barrier, inc=1, device_id={"sp": s + 1}, device_id_type=MESH)

    pl.semaphore_signal(barrier, inc=1, device_id={"tp": other}, device_id_type=MESH)


    for load in loads[:3]:
        load.wait()
    lk[0, pl.ds(0, leak_t.shape[0]), :] = leak_t[...]
    x = tokv[...].astype(F32)
    center = x - jnp.mean(x, axis=-1, keepdims=True)
    spread = jnp.mean(center * center, axis=-1, keepdims=True)
    rows[0, pl.ds(pl.multiple_of(t * half, half), half), :] = (
        center * lax.rsqrt(spread + 1e-05) * gain[...]
    ).astype(BF)

    ends = jnp.where(has_left, 1, 0) + jnp.where(has_right, 1, 0)
    pl.semaphore_wait(barrier, nf + ends)


    def own_right(p):
        return remote(wblock(s, p), wblock(s, p), zs.at[s, p], zr.at[s, p], sp=s + 1)

    def own_left(p):
        return remote(wblock(s, p), wblock(s, p), zsl.at[p], zr.at[s, p], sp=s - 1)

    def relay(b, p, to):
        return remote(wblock(b, p), wblock(b, p), zs.at[b, p], zr.at[b, p], sp=to)

    def send_own(p, where):
        @pl.when(where & has_right)
        def _():
            own_right(p).start()

        @pl.when(where & has_left)
        def _():
            own_left(p).start()

    def zhop(k, p):
        @pl.when((s - k >= 0) & has_right)
        def _():
            relay(s - k, p, s + 1).wait_recv()
            relay(s - k, p, s + 1).start()

        @pl.when((s + k < ns) & has_left)
        def _():
            relay(s + k, p, s - 1).wait_recv()
            relay(s + k, p, s - 1).start()

    def zready(p):
        def far(k, carry):
            zhop(k, p)
            return carry

        if ns > 3:
            lax.fori_loop(3, ns, far, 0)

        def hop(k, carry):
            @pl.when((s - k >= 0) & (s == ns - 1))
            def _():
                relay(s - k, p, s - 1).wait_recv()

            @pl.when((s + k < ns) & (s == 0))
            def _():
                relay(s + k, p, s + 1).wait_recv()

            return carry

        lax.fori_loop(1, ns, hop, 0)

    always = s >= 0
    for p in range(2):
        wload(p).wait()
        send_own(p, always)

    quarter = half // 2

    def piece(d, j):
        return rows.at[d, pl.ds(pl.multiple_of(t * half + j * quarter, quarter), quarter), :]

    def core_rows(d, core):
        return rows.at[d, pl.ds(pl.multiple_of(core * half, half), half), :]

    def row_send(d, j, to_d, slot):
        return remote(piece(d, j), piece(d ^ to_d, j), rs.at[slot], rr.at[d ^ to_d, j], fs=f ^ to_d)

    def row_arrived(d, j):
        remote(piece(d, j), piece(d, j), rs.at[0], rr.at[d, j], fs=f ^ 1).wait_recv()

    def twin(d):
        return remote(core_rows(d, t), core_rows(d, t), ts.at[d], tr.at[d], tp=other)

    def twin_arrived(d):
        remote(core_rows(d, other), core_rows(d, other), ts.at[d], tr.at[d], tp=other).wait_recv()

    def leak_send(d):
        return remote(lk.at[0], lk.at[d], ls.at[d], lr.at[d], fs=f ^ d)

    def leak_arrived(d):
        remote(lk.at[d], lk.at[d], ls.at[d], lr.at[d], fs=f ^ 1).wait_recv()

    for d in range(1, nf):
        leak_send(d).start()
    row_send(0, 0, 1, 0).start()
    row_send(0, 1, 2, 1).start()
    row_send(0, 1, 1, 2).start()
    row_send(0, 0, 2, 3).start()
    twin(0).start()
    for p in range(2, np_):
        wload(p).wait()
        send_own(p, jnp.logical_not(inner))

    zhop(1, 0)
    zhop(1, 1)


    for d in range(1, nf):
        leak_arrived(d)
    ri = lax.broadcasted_iota(jnp.int32, (length, length), 0)
    ci = lax.broadcasted_iota(jnp.int32, (length, length), 1)
    tril = (ri >= ci).astype(F32)
    triu = (ri <= ci).astype(F32)
    high = lax.Precision.HIGHEST
    head_leak = jnp.concatenate(
        [lk[d, pl.ds(f, 1), :] for d in range(nf)] + [jnp.zeros((8 - nf, length), F32)], axis=0
    )
    lsum = lax.dot_general(tril, head_leak, NT, precision=high, preferred_element_type=F32)
    lsum_t = jnp.dot(head_leak, triu, precision=high, preferred_element_type=F32)
    for d in range(nf):
        lcol[d] = jnp.broadcast_to(lsum[:, d : d + 1], (length, wide))
        lrow[d] = jnp.broadcast_to(lsum_t[d : d + 1, :], (8, length))

    zhop(2, 0)
    send_own(2, inner)


    pw = cols // 4

    def opiece(d, q):
        return wo.at[d, :, pl.ds(pl.multiple_of(q * pw, pw), pw)]

    def order(to_d, i):
        first = 2 * odd + (1 if to_d == 1 else 0)
        second = 2 * odd + (0 if to_d == 1 else 1)
        return (first, second, 2 - 2 * odd, 3 - 2 * odd)[i]

    def own_out(to_d, i):
        q = order(to_d, i)
        return remote(opiece(0, q), opiece(to_d, q), os_.at[to_d, i], or_.at[to_d, q], fs=f ^ to_d)

    def out_arrived(d, q):
        remote(opiece(d, q), opiece(d, q), os_.at[1, 0], or_.at[d, q], fs=f ^ 1).wait_recv()

    def relay_out(d, to_d):
        q = order(d, 0)
        return remote(opiece(d, q), opiece(3, q), rl.at[to_d], or_.at[3, q], fs=f ^ to_d)

    def assist(i):
        q = 2 * odd + i
        return remote(opiece(3, q), opiece(3, q), za.at[i], or_.at[3, q], sp=mate)

    row_arrived(1, 0)
    row_send(1, 0, 2, 4).start()
    row_arrived(2, 1)
    row_send(2, 1, 1, 5).start()
    for j in range(2):
        oload(j).wait()
    for i in range(2):
        own_out(1, i).start()
        own_out(2, i).start()

    zhop(1, 2)
    zhop(2, 1)
    zhop(2, 2)
    send_own(3, inner)
    row_arrived(1, 1)
    twin(1).start()
    row_arrived(2, 0)
    twin(2).start()
    zhop(1, 3)
    send_own(4, inner)

    def project(d, n, p, q):
        left = rows[d : d + n].reshape(n * length, rows.shape[2])
        co = pl.ds(p * wide, (q - p) * wide)
        made = jnp.dot(left, wg[:, co], preferred_element_type=F32).astype(BF)
        y[d : d + n, :, co] = made.reshape(n, length, (q - p) * wide)

    def group(d, p):
        return y[d, :, p * wide : (p + 1) * wide]

    causal = ri >= ci
    tril_short = tril.astype(BF)

    def local(d):
        fl = floor[f]
        logits = group(d, FORGET).astype(F32)
        retain = fl + (1.0 - fl) * jax.nn.sigmoid(logits)
        keys = (1.0 - fl) * jax.nn.sigmoid(-logits)
        step = jnp.log(retain)
        coarse = step.astype(BF)
        fine = (step - coarse.astype(F32)).astype(BF)
        both = jnp.dot(
            tril_short, jnp.concatenate([coarse, fine], axis=1), preferred_element_type=F32
        )
        total = both[:, :wide] + both[:, wide:]
        raw = group(d, QUERY).astype(F32)
        query = raw * jax.nn.sigmoid(raw) * jnp.exp(total)
        value = group(d, VALUE)
        scores = lax.dot_general(
            query.astype(BF), (keys * jnp.exp(-total)).astype(BF), NT, preferred_element_type=F32
        )
        lc = lcol[d]
        gap = lc[:, 0:1] - lrow[d, 0:1, :]
        scores = jnp.where(causal, scores * jnp.exp(jnp.where(causal, gap, 0.0)), 0.0)
        inside[d] = jnp.dot(scores.astype(BF), value, preferred_element_type=F32)
        reach[d] = (query * jnp.exp(lc)).astype(BF)
        full = total + lc
        end = full[length - 1 :, :]
        update = (keys * jnp.exp(end - full)).astype(BF)
        states[d] = lax.dot_general(value, update, TN, preferred_element_type=F32)
        sdecay[d] = jnp.broadcast_to(jnp.exp(end), (8, wide))

    def many(body, first, last):
        def one(d, carry):
            body(d)
            return carry

        lax.fori_loop(first, last, one, 0)

    for load in loads[3:]:
        load.wait()
    twin_arrived(0)
    zready(0)
    zready(1)
    project(0, 1, 0, 2)
    twin_arrived(1)
    twin_arrived(2)
    project(1, 2, 0, 2)
    zhop(1, 4)
    zready(2)
    project(0, 1, 2, 3)
    zhop(2, 3)
    project(1, 2, 2, 3)
    zhop(2, 4)
    row_arrived(3, 0)
    row_arrived(3, 1)
    twin(3).start()
    many(local, 0, 3)
    twin_arrived(3)
    project(3, 1, 0, 2)
    project(3, 1, 2, 3)
    many(local, 3, 4)

    out_arrived(2, order(2, 0))
    relay_out(2, 1).start()
    out_arrived(1, order(1, 0))
    relay_out(1, 2).start()
    own_out(1, 2).start()
    own_out(2, 2).start()

    def state_copy(d):
        return remote(sout.at[d], sin.at[d], ss.at[d], sr.at[d], sp=s + 1)

    def place(j, g):
        return mix.at[:, pl.ds(pl.multiple_of(j * depth + g * wide, wide), wide)]

    def mixed_send(d, j):
        return remote(msend.at[d, j], place(j, f), xs.at[d, j], xr.at[d, j], fs=f ^ d)

    def mixed_arrived(d, j):
        remote(msend.at[d, j], place(j, f ^ d), xs.at[d, j], xr.at[d, j], fs=f ^ 1).wait_recv()

    def deliver(d, j, value):
        if d == 0:
            mix[:, pl.ds(pl.multiple_of(j * depth + f * wide, wide), wide)] = value
        else:
            msend[d, j] = value
            mixed_send(d, j).start()

    def chain(d):
        @pl.when(has_left)
        def _():
            state_copy(d).wait_recv()

        @pl.when(s == 0)
        def _():
            sin[d] = jnp.zeros(sin.shape[1:], BF)

        @pl.when(has_right)
        def _():
            sout[d] = (sin[d].astype(F32) * sdecay[d, 0:1, :] + states[d]).astype(BF)
            state_copy(d).start()

        raw = inside[d] + lax.dot_general(reach[d], sin[d], NT, preferred_element_type=F32)
        scale = lax.rsqrt(jnp.mean(raw * raw, axis=-1, keepdims=True) + 1e-06)
        deliver(d, 1, (raw * scale * hgain[...]).astype(BF))

    turns = (3, 1, 2, 0)
    for d in turns:
        chain(d)


    edge = rim.shape[1]

    def rim_copy(d):
        return remote(
            y.at[d, pl.ds(length - edge, edge), pl.ds(SIGNAL * wide, wide)], rim.at[d],
            ms.at[d], mr.at[d], sp=s + 1,
        )

    zready(3)
    for d in turns:
        project(d, 1, 3, 4)

        @pl.when(has_right)
        def _(d=d):
            rim_copy(d).start()

        @pl.when(s == 0)
        def _(d=d):
            rim[d] = jnp.zeros((edge, wide), BF)

    def filtering(d):
        @pl.when(has_left)
        def _():
            rim_copy(d).wait_recv()

        padded = jnp.concatenate([rim[d], group(d, SIGNAL)], axis=0).astype(F32)
        margin = taps.shape[1] - 1
        filtered = jnp.zeros((length, wide), F32)
        for o in range(margin + 1):
            start = edge - margin + o
            filtered = filtered + taps[f, o : o + 1, :] * padded[start : start + length]
        filt[d] = filtered

    many(filtering, 0, nf)
    zready(4)
    for i in range(2):
        out_arrived(3, 2 * odd + i)
        assist(i).start()
    for d in turns:
        project(d, 1, 4, 5)
        deliver(d, 0, (group(d, GATE).astype(F32) * filt[d]).astype(BF))
    own_out(1, 3).start()
    own_out(2, 3).start()


    def share(i):
        return remote(
            acc.at[i, pl.ds(pl.multiple_of(other * half, half), half), :], orecv.at[i], es.at[i], er.at[i], tp=other
        )

    for d in (1, 2, 3):
        for j in (1, 0):
            mixed_arrived(d, j)

    def begin(i, d, c):
        co = pl.ds(pl.multiple_of(c * 2 * pw, 2 * pw), 2 * pw)
        acc[i] = jnp.dot(mix[...], wo[d, :, co], preferred_element_type=F32)
        share(i).start()

    def finish(i, d, c):
        share(i).wait_recv()
        at = pl.ds(pl.multiple_of((f ^ d) * cols + c * 2 * pw, 2 * pw), 2 * pw)
        out[0, :, at] = (acc[i, pl.ds(pl.multiple_of(t * half, half), half), :] + orecv[i]).astype(BF)

    plan = [
        (0, odd, ()),
        (0, 1 - odd, ()),
        (1, odd, (order(1, 1),)),
        (2, odd, (order(2, 1),)),
        (3, odd, ()),
        (3, 1 - odd, (2 - 2 * odd, 3 - 2 * odd)),
        (1, 1 - odd, (2 - 2 * odd, 3 - 2 * odd)),
        (2, 1 - odd, (2 - 2 * odd, 3 - 2 * odd)),
    ]
    for i, (d, c, waits) in enumerate(plan):
        for q in waits:
            out_arrived(d, q)
        begin(i, d, c)
        if i:
            finish(i - 1, *plan[i - 1][:2])
    finish(len(plan) - 1, *plan[-1][:2])


    for p in range(np_):
        def drained(b, carry, p=p):
            @pl.when(((b < s) & has_right) | ((b > s) & has_left))
            def _():
                relay(b, p, s).wait_send()

            return carry

        lax.fori_loop(0, ns, drained, 0)

        @pl.when(has_right)
        def _(p=p):
            own_right(p).wait_send()

        @pl.when(has_left)
        def _(p=p):
            own_left(p).wait_send()

    for d, j, to_d, slot in ((0, 0, 1, 0), (0, 1, 2, 1), (0, 1, 1, 2), (0, 0, 2, 3), (1, 0, 2, 4), (2, 1, 1, 5)):
        row_send(d, j, to_d, slot).wait_send()
    for to_d in range(1, 3):
        for i in range(4):
            own_out(to_d, i).wait_send()
        relay_out(3 - to_d, to_d).wait_send()
    for i in range(2):
        assist(i).wait_send()
    for d in range(nf):
        twin(d).wait_send()
        if d:
            leak_send(d).wait_send()
            for j in range(2):
                mixed_send(d, j).wait_send()
    for i in range(len(plan)):
        share(i).wait_send()

    @pl.when(has_right)
    def _():
        for d in range(nf):
            state_copy(d).wait_send()
            rim_copy(d).wait_send()


def body(ns, nf, tokens, norm_gain, w0, w1, w2, w3, w4, conv_taps, floor_gate, leak, head_gain, cow, how):
    half, width = tokens.shape[1:]
    length = 2 * half
    heads = leak.shape[2]
    kd = w0.shape[0]
    wide = w0.shape[1] // nf
    assert heads == nf and nf == 4 and floor_gate.shape[0] == heads * wide and ns % 2 == 0
    taps = conv_taps.reshape(conv_taps.shape[0], nf, wide).transpose(1, 0, 2)
    vm = pl.BlockSpec(memory_space=pltpu.VMEM)
    hbm = pl.BlockSpec(memory_space=pltpu.HBM)
    dma = pltpu.SemaphoreType.DMA
    depth, cols = cow.shape
    scratch = [
        pltpu.VMEM((half, width), BF),
        pltpu.VMEM((1, width), F32),
        pltpu.VMEM(taps.shape, F32),
        pltpu.VMEM((heads, 1, wide), F32),
        pltpu.VMEM((heads, length), F32),
        pltpu.VMEM((1, wide), F32),
        pltpu.VMEM((nf, length, width), BF),
        pltpu.VMEM((ns * kd, 5 * wide), BF),
        pltpu.VMEM((nf, length, 5 * wide), BF),
        pltpu.VMEM((nf, 2 * depth, cols), BF),
        pltpu.VMEM((nf, 16, wide), BF),
        pltpu.VMEM((nf, length, wide), F32),
        pltpu.VMEM((nf, length, wide), F32),
        pltpu.VMEM((nf, length, wide), BF),
        pltpu.VMEM((nf, wide, wide), F32),
        pltpu.VMEM((nf, 8, wide), F32),
        pltpu.VMEM((nf, wide, wide), BF),
        pltpu.VMEM((nf, wide, wide), BF),
        pltpu.VMEM((nf, 8, length), F32),
        pltpu.VMEM((nf, length, wide), F32),
        pltpu.VMEM((nf, 8, length), F32),
        pltpu.VMEM((nf, 2, length, wide), BF),
        pltpu.VMEM((length, 2 * depth), BF),
        pltpu.VMEM((2 * nf, length, cols // 2), F32),
        pltpu.VMEM((2 * nf, half, cols // 2), F32),
        dma((6,)), dma((ns, 5)), dma((5,)), dma((ns, 5)), dma((5,)),
        dma((6,)), dma((nf, 2)), dma((nf,)), dma((nf,)), dma((nf,)), dma((nf,)),
        dma((2,)), dma((3, 4)), dma((nf, 4)), dma((3,)), dma((2,)),
        dma((nf, 2)), dma((nf, 2)), dma((nf,)), dma((nf,)), dma((nf,)), dma((nf,)),
        dma((2 * nf,)), dma((2 * nf,)),
    ]
    return pl.pallas_call(
        functools.partial(kernel, ns, nf),
        out_shape=jax.ShapeDtypeStruct(tokens.shape, BF),
        in_specs=[hbm] * 13,
        out_specs=vm,
        scratch_shapes=scratch,
        compiler_params=pltpu.CompilerParams(
            collective_id=0, has_side_effects=True, vmem_limit_bytes=60 * 2**20
        ),
    )(
        tokens, norm_gain[None], w0, w1, w2, w3, w4, taps, floor_gate.reshape(heads, 1, wide),
        leak[0].T, head_gain[None], cow, how,
    )


def solution(mesh):
    in_specs = (
        P("fs", ("sp", "tp"), None),
        P(),
        P("sp", "tp"),
        P("sp", "tp"),
        P("sp", "tp"),
        P("sp", "tp"),
        P("sp", "tp"),
        P(None, "tp"),
        P("tp"),
        P("fs", "sp", "tp"),
        P(),
        P("tp", "fs"),
        P("tp", "fs"),
    )
    out_specs = P("fs", ("sp", "tp"), None)
    step = functools.partial(body, mesh.shape["sp"], mesh.shape["fs"])
    return jax.shard_map(step, mesh=mesh, in_specs=in_specs, out_specs=out_specs, check_vma=False)
```

time: 87.1 us -> 75.5 us (0.87)
  local copies, waits for them, and re-layouts: 12.1 us -> 2.09 us
  Pallas kernels: 74.4 us -> 73 us
    unnamed x27 -> x1, local copies, waits for them, and re-layouts: 12.1 us -> 2.09 us
    pallas_call x1, Pallas kernels: 74.4 us -> 73 us  [body(): pl.pallas_call(functools.partial(kernel, ns, nf), out_shape=jax.ShapeDtyp...]
where the time goes in v2:
time: 75.5 us; the launch traced here: 75.1 us
  Pallas kernels  73 us (97%)
  local copies, waits for them, and re-layouts  2.09 us (3%)
    pallas_call x1, Pallas kernels, body(): pl.pallas_call(functools.partial(kernel, ns, nf), out_shape=jax.ShapeDtyp...  73 us
    unnamed x1, local copies, waits for them, and re-layouts  2.09 us

profile of v2, /device:TPU:9, one launch (start us, length us, event | category | flops | bytes accessed | tf_op | source)
XLA Modules:
  0.0 75.1 jit_solution(9913125110444881767)
XLA Ops:
  0.0 73.0 %shard_map.127 = bf16[1,192,2048]{2,1,0:T(8,128)(2,1)} custom-call(bf16[1,192,2048]{2,1,0:T(8,128)(2,1)} %tok_h.1, f32[1,2048]{1,0:T(1,128)} %bitcast.9, bf16[512,512]{1,0:T(8,128)(2,1)} %w0.1, bf16[512,512]{1,0:T(8,128)(2,1)} %w1.1, bf16[512,512]{1,0:T(8,128)(2,1)} %w2.1, bf16[512,512]{1,0:T(8,128)(2,1)} %w3.1, bf16[512,512]{1,0:T(8,128)(2,1)} %w4.1, ...), custom_call_target="tpu_custom_call" | custom-call | tf_op jit(solution)/shard_map/pallas_call | solution.py:558
  73.0 2.1 %copy.15 = bf16[1,192,2048]{2,1,0:T(8,128)(2,1)} copy(bf16[1,192,2048]{2,1,0:T(8,128)(2,1)} %shard_map.127) | data formatting | bytes 1572864

commit v3 on v2

--- a/solution.py
+++ b/solution.py
@@ -20,9 +20,9 @@
     tok_h, gain_h, w0, w1, w2, w3, w4, taps_h, floor_h, leak_h, hgain_h, cow, how,
     out,
     tokv, gain, taps, floor, leak_t, hgain,
-    rows, wg, y, wo, rim, filt, inside, reach, states, sdecay, sin, sout,
-    lk, lcol, lrow, msend, mix, acc, orecv,
-    il, zs, zsl, zr, zloc, rs, rr, ts, tr, ls, lr, oloc, os_, or_, rl, za, xs, xr, ms, mr, ss, sr, es, er,
+    rows, wg, y, wo, brim, rim, filt, inside, reach, states, sdecay, sin, sout,
+    lk, lcol, lrow, msend, mix, acc, orecv, done,
+    il, zs, zsl, zr, zloc, rs, rr, ts, tr, ls, lr, oloc, os_, or_, ov, zc, xs, xr, ms, mr, ss, sr, es, er, fin,
 ):
     s, f, t = lax.axis_index("sp"), lax.axis_index("fs"), lax.axis_index("tp")
     other = 1 - t
@@ -55,7 +55,7 @@
         )
 
     def oload(j):
-        return pltpu.make_async_copy(outs[j], wo.at[0, pl.ds(j * depth, depth), :], oloc.at[j])
+        return pltpu.make_async_copy(outs[j], wo.at[0, pl.ds(j * depth, depth), :], oloc.at[0])
 
     loads = [
         pltpu.make_async_copy(src, dst, il.at[i])
@@ -104,13 +104,13 @@
 
 
     def own_right(p):
-        return remote(wblock(s, p), wblock(s, p), zs.at[s, p], zr.at[s, p], sp=s + 1)
+        return remote(wblock(s, p), wblock(s, p), zs.at[0], zr.at[s, p], sp=s + 1)
 
     def own_left(p):
-        return remote(wblock(s, p), wblock(s, p), zsl.at[p], zr.at[s, p], sp=s - 1)
+        return remote(wblock(s, p), wblock(s, p), zsl.at[0], zr.at[s, p], sp=s - 1)
 
     def relay(b, p, to):
-        return remote(wblock(b, p), wblock(b, p), zs.at[b, p], zr.at[b, p], sp=to)
+        return remote(wblock(b, p), wblock(b, p), zs.at[0], zr.at[b, p], sp=to)
 
     def send_own(p, where):
         @pl.when(where & has_right)
@@ -166,30 +166,27 @@
     def core_rows(d, core):
         return rows.at[d, pl.ds(pl.multiple_of(core * half, half), half), :]
 
-    def row_send(d, j, to_d, slot):
-        return remote(piece(d, j), piece(d ^ to_d, j), rs.at[slot], rr.at[d ^ to_d, j], fs=f ^ to_d)
+    def row_send(d, j, to_d):
+        return remote(piece(d, j), piece(d ^ to_d, j), rs.at[0], rr.at[(d ^ to_d) - 1, j], fs=f ^ to_d)
 
     def row_arrived(d, j):
-        remote(piece(d, j), piece(d, j), rs.at[0], rr.at[d, j], fs=f ^ 1).wait_recv()
+        remote(piece(d, j), piece(d, j), rs.at[0], rr.at[d - 1, j], fs=f ^ 1).wait_recv()
 
     def twin(d):
-        return remote(core_rows(d, t), core_rows(d, t), ts.at[d], tr.at[d], tp=other)
+        return remote(core_rows(d, t), core_rows(d, t), ts.at[0], tr.at[d], tp=other)
 
     def twin_arrived(d):
-        remote(core_rows(d, other), core_rows(d, other), ts.at[d], tr.at[d], tp=other).wait_recv()
+        remote(core_rows(d, other), core_rows(d, other), ts.at[0], tr.at[d], tp=other).wait_recv()
 
     def leak_send(d):
-        return remote(lk.at[0], lk.at[d], ls.at[d], lr.at[d], fs=f ^ d)
-
-    def leak_arrived(d):
-        remote(lk.at[d], lk.at[d], ls.at[d], lr.at[d], fs=f ^ 1).wait_recv()
+        return remote(lk.at[0], lk.at[d], ls.at[0], lr.at[0], fs=f ^ d)
 
     for d in range(1, nf):
         leak_send(d).start()
-    row_send(0, 0, 1, 0).start()
-    row_send(0, 1, 2, 1).start()
-    row_send(0, 1, 1, 2).start()
-    row_send(0, 0, 2, 3).start()
+    row_send(0, 0, 1).start()
+    row_send(0, 1, 2).start()
+    row_send(0, 1, 1).start()
+    row_send(0, 0, 2).start()
     twin(0).start()
     for p in range(2, np_):
         wload(p).wait()
@@ -199,8 +196,8 @@
     zhop(1, 1)
 
 
-    for d in range(1, nf):
-        leak_arrived(d)
+    others = lk.at[pl.ds(1, nf - 1)]
+    remote(others, others, ls.at[0], lr.at[0], fs=f ^ 1).wait_recv()
     ri = lax.broadcasted_iota(jnp.int32, (length, length), 0)
     ci = lax.broadcasted_iota(jnp.int32, (length, length), 1)
     tril = (ri >= ci).astype(F32)
@@ -221,35 +218,63 @@
 
     pw = cols // 4
 
-    def opiece(d, q):
-        return wo.at[d, :, pl.ds(pl.multiple_of(q * pw, pw), pw)]
+    full = (0, 2 * depth)
+
+    def opiece(d, q, part=full):
+        return wo.at[d, pl.ds(*part), pl.ds(pl.multiple_of(q * pw, pw), pw)]
 
     def order(to_d, i):
-        first = 2 * odd + (1 if to_d == 1 else 0)
-        second = 2 * odd + (0 if to_d == 1 else 1)
-        return (first, second, 2 - 2 * odd, 3 - 2 * odd)[i]
-
-    def own_out(to_d, i):
+        low, high = 2 * odd, 2 - 2 * odd
+        return ((low + 1, low, high, high + 1) if to_d == 1 else (low, low + 1, high + 1, high))[i]
+
+    lower, upper = (0, depth), (depth, depth)
+
+    def own_out(to_d, i, part=full):
         q = order(to_d, i)
-        return remote(opiece(0, q), opiece(to_d, q), os_.at[to_d, i], or_.at[to_d, q], fs=f ^ to_d)
-
-    def out_arrived(d, q):
-        remote(opiece(d, q), opiece(d, q), os_.at[1, 0], or_.at[d, q], fs=f ^ 1).wait_recv()
+        return remote(opiece(0, q, part), opiece(to_d, q, part), os_.at[0], or_.at[to_d - 1, q], fs=f ^ to_d)
+
+    def out_arrived(d, q, part=full):
+        remote(opiece(d, q, part), opiece(d, q, part), os_.at[0], or_.at[d - 1, q], fs=f ^ 1).wait_recv()
+
+    def third_upper(to_d):
+        q = order(to_d, 2)
+        return remote(opiece(0, q, upper), opiece(to_d, q, upper), os_.at[0], ov.at[to_d - 1], fs=f ^ to_d)
+
+    def third_lower(to_d):
+        return own_out(to_d, 2, lower)
+
+    taken = (depth, depth // 2)
+
+    def fourth(to_d, side):
+        return own_out(to_d, 3, (taken[side], 2 * depth - taken[side]))
+
+    def swap(d, side):
+        q, part = order(d, 0), (0, taken[1 - side])
+        return remote(opiece(d, q, part), opiece(d, q, part), os_.at[0], zc.at[d - 1], sp=mate)
+
+    def swapped(d, side):
+        q, part = order(d, 3), (0, taken[side])
+        remote(opiece(d, q, part), opiece(d, q, part), os_.at[0], zc.at[d - 1], sp=mate).wait_recv()
+
+    def by_side(work):
+        for side in range(2):
+            @pl.when(odd == side)
+            def _(side=side):
+                work(side)
 
     def relay_out(d, to_d):
         q = order(d, 0)
-        return remote(opiece(d, q), opiece(3, q), rl.at[to_d], or_.at[3, q], fs=f ^ to_d)
+        return remote(opiece(d, q), opiece(3, q), os_.at[0], or_.at[2, q], fs=f ^ to_d)
 
     def assist(i):
         q = 2 * odd + i
-        return remote(opiece(3, q), opiece(3, q), za.at[i], or_.at[3, q], sp=mate)
+        return remote(opiece(3, q), opiece(3, q), os_.at[0], or_.at[2, q], sp=mate)
 
     row_arrived(1, 0)
-    row_send(1, 0, 2, 4).start()
+    row_send(1, 0, 2).start()
     row_arrived(2, 1)
-    row_send(2, 1, 1, 5).start()
-    for j in range(2):
-        oload(j).wait()
+    row_send(2, 1, 1).start()
+    pltpu.make_async_copy(wo.at[0], wo.at[0], oloc.at[0]).wait()
     for i in range(2):
         own_out(1, i).start()
         own_out(2, i).start()
@@ -266,10 +291,10 @@
     send_own(4, inner)
 
     def project(d, n, p, q):
-        left = rows[d : d + n].reshape(n * length, rows.shape[2])
+        left = rows[pl.ds(d, n)].reshape(n * length, rows.shape[2])
         co = pl.ds(p * wide, (q - p) * wide)
         made = jnp.dot(left, wg[:, co], preferred_element_type=F32).astype(BF)
-        y[d : d + n, :, co] = made.reshape(n, length, (q - p) * wide)
+        y[pl.ds(d, n), :, co] = made.reshape(n, length, (q - p) * wide)
 
     def group(d, p):
         return y[d, :, p * wide : (p + 1) * wide]
@@ -322,16 +347,16 @@
     twin_arrived(1)
     twin_arrived(2)
     project(1, 2, 0, 2)
-    zhop(1, 4)
     zready(2)
     project(0, 1, 2, 3)
-    zhop(2, 3)
     project(1, 2, 2, 3)
-    zhop(2, 4)
     row_arrived(3, 0)
     row_arrived(3, 1)
     twin(3).start()
     many(local, 0, 3)
+    zhop(1, 4)
+    zhop(2, 3)
+    zhop(2, 4)
     twin_arrived(3)
     project(3, 1, 0, 2)
     project(3, 1, 2, 3)
@@ -341,26 +366,21 @@
     relay_out(2, 1).start()
     out_arrived(1, order(1, 0))
     relay_out(1, 2).start()
-    own_out(1, 2).start()
-    own_out(2, 2).start()
 
     def state_copy(d):
-        return remote(sout.at[d], sin.at[d], ss.at[d], sr.at[d], sp=s + 1)
+        return remote(sout.at[d], sin.at[d], ss.at[0], sr.at[d], sp=s + 1)
 
     def place(j, g):
         return mix.at[:, pl.ds(pl.multiple_of(j * depth + g * wide, wide), wide)]
 
     def mixed_send(d, j):
-        return remote(msend.at[d, j], place(j, f), xs.at[d, j], xr.at[d, j], fs=f ^ d)
-
-    def mixed_arrived(d, j):
-        remote(msend.at[d, j], place(j, f ^ d), xs.at[d, j], xr.at[d, j], fs=f ^ 1).wait_recv()
+        return remote(msend.at[d - 1, j], place(j, f), xs.at[0], xr.at[0], fs=f ^ d)
 
     def deliver(d, j, value):
         if d == 0:
             mix[:, pl.ds(pl.multiple_of(j * depth + f * wide, wide), wide)] = value
         else:
-            msend[d, j] = value
+            msend[d - 1, j] = value
             mixed_send(d, j).start()
 
     def chain(d):
@@ -382,35 +402,84 @@
         deliver(d, 1, (raw * scale * hgain[...]).astype(BF))
 
     turns = (3, 1, 2, 0)
+    last = s == ns - 1
+    inland = jnp.logical_not(last)
+
+
+    edge = rim.shape[1]
+
+    def rim_copy():
+        return remote(brim, rim, ms.at[0], mr.at[0], sp=s + 1)
+
+    def swaps(side):
+        for d in (1, 2):
+            swap(d, side).start()
+
+    def signal():
+        zready(3)
+
+        @pl.when(has_right)
+        def _():
+            ends_ = rows[:, pl.ds(length - edge, edge), :].reshape(nf * edge, rows.shape[2])
+            made = jnp.dot(ends_, wg[:, pl.ds(SIGNAL * wide, wide)], preferred_element_type=F32).astype(BF)
+            brim[...] = made.reshape(nf, edge, wide)
+            rim_copy().start()
+
+        @pl.when(s == 0)
+        def _():
+            rim[...] = jnp.zeros(rim.shape, BF)
+
+        @pl.when((odd == 0) & (s > 0))
+        def _():
+            swaps(0)
+
+        def one(d, carry):
+            project(d, 1, 3, 4)
+            return carry
+
+        lax.fori_loop(0, nf, one, 0)
+
+    def assists():
+        for i in range(2):
+            out_arrived(3, 2 * odd + i)
+            assist(i).start()
+
+    @pl.when(odd == 1)
+    def _():
+        swaps(1)
+
+    def thirds():
+        for to_d in (1, 2):
+            third_upper(to_d).start()
+
+    @pl.when(last)
+    def _():
+        thirds()
+        signal()
+        assists()
+
     for d in turns:
         chain(d)
 
-
-    edge = rim.shape[1]
-
-    def rim_copy(d):
-        return remote(
-            y.at[d, pl.ds(length - edge, edge), pl.ds(SIGNAL * wide, wide)], rim.at[d],
-            ms.at[d], mr.at[d], sp=s + 1,
-        )
-
-    zready(3)
-    for d in turns:
-        project(d, 1, 3, 4)
-
-        @pl.when(has_right)
-        def _(d=d):
-            rim_copy(d).start()
-
-        @pl.when(s == 0)
-        def _(d=d):
-            rim[d] = jnp.zeros((edge, wide), BF)
+    @pl.when(s == 0)
+    def _():
+        swaps(0)
+
+    @pl.when(inland)
+    def _():
+        thirds()
+        signal()
+
+    @pl.when(inland)
+    def _():
+        assists()
+
+
+    @pl.when(has_left)
+    def _():
+        rim_copy().wait_recv()
 
     def filtering(d):
-        @pl.when(has_left)
-        def _():
-            rim_copy(d).wait_recv()
-
         padded = jnp.concatenate([rim[d], group(d, SIGNAL)], axis=0).astype(F32)
         margin = taps.shape[1] - 1
         filtered = jnp.zeros((length, wide), F32)
@@ -421,24 +490,26 @@
 
     many(filtering, 0, nf)
     zready(4)
-    for i in range(2):
-        out_arrived(3, 2 * odd + i)
-        assist(i).start()
     for d in turns:
         project(d, 1, 4, 5)
         deliver(d, 0, (group(d, GATE).astype(F32) * filt[d]).astype(BF))
-    own_out(1, 3).start()
-    own_out(2, 3).start()
+    for to_d in (1, 2):
+        third_lower(to_d).start()
+
+    def fourths(side):
+        for to_d in (1, 2):
+            fourth(to_d, side).start()
+
+    by_side(fourths)
 
 
     def share(i):
         return remote(
-            acc.at[i, pl.ds(pl.multiple_of(other * half, half), half), :], orecv.at[i], es.at[i], er.at[i], tp=other
+            acc.at[i, pl.ds(pl.multiple_of(other * half, half), half), :], orecv.at[i], es.at[0], er.at[i], tp=other
         )
 
-    for d in (1, 2, 3):
-        for j in (1, 0):
-            mixed_arrived(d, j)
+    mixed = remote(msend, msend, xs.at[0], xr.at[0], fs=f ^ 1)
+    mixed.wait_recv()
 
     def begin(i, d, c):
         co = pl.ds(pl.multiple_of(c * 2 * pw, 2 * pw), 2 * pw)
@@ -448,67 +519,82 @@
     def finish(i, d, c):
         share(i).wait_recv()
         at = pl.ds(pl.multiple_of((f ^ d) * cols + c * 2 * pw, 2 * pw), 2 * pw)
-        out[0, :, at] = (acc[i, pl.ds(pl.multiple_of(t * half, half), half), :] + orecv[i]).astype(BF)
-
+        done[:, at] = (acc[i, pl.ds(pl.multiple_of(t * half, half), half), :] + orecv[i]).astype(BF)
+        store(i, d, c).start()
+
+    def store(i, d, c):
+        at = pl.ds(pl.multiple_of((f ^ d) * cols + c * 2 * pw, 2 * pw), 2 * pw)
+        return pltpu.make_async_copy(done.at[:, at], out.at[0, :, at], fin.at[0])
+
+    def last_quarters(d):
+        third_upper(d).wait_recv()
+        out_arrived(d, order(d, 2), lower)
+
+        def rest(side):
+            swapped(d, side)
+            out_arrived(d, order(d, 3), (taken[side], 2 * depth - taken[side]))
+
+        by_side(rest)
+
+    def assisted(d):
+        for q in (2 - 2 * odd, 3 - 2 * odd):
+            out_arrived(3, q)
+
+    lag = 3
     plan = [
-        (0, odd, ()),
-        (0, 1 - odd, ()),
-        (1, odd, (order(1, 1),)),
-        (2, odd, (order(2, 1),)),
-        (3, odd, ()),
-        (3, 1 - odd, (2 - 2 * odd, 3 - 2 * odd)),
-        (1, 1 - odd, (2 - 2 * odd, 3 - 2 * odd)),
-        (2, 1 - odd, (2 - 2 * odd, 3 - 2 * odd)),
+        (0, odd, None),
+        (0, 1 - odd, None),
+        (1, odd, lambda d: out_arrived(d, order(d, 1))),
+        (2, odd, lambda d: out_arrived(d, order(d, 1))),
+        (3, odd, None),
+        (1, 1 - odd, last_quarters),
+        (2, 1 - odd, last_quarters),
+        (3, 1 - odd, assisted),
     ]
-    for i, (d, c, waits) in enumerate(plan):
-        for q in waits:
-            out_arrived(d, q)
+    for i, (d, c, ready) in enumerate(plan):
+        if ready:
+            ready(d)
         begin(i, d, c)
-        if i:
-            finish(i - 1, *plan[i - 1][:2])
-    finish(len(plan) - 1, *plan[-1][:2])
-
-
-    for p in range(np_):
-        def drained(b, carry, p=p):
-            @pl.when(((b < s) & has_right) | ((b > s) & has_left))
-            def _():
-                relay(b, p, s).wait_send()
-
-            return carry
-
-        lax.fori_loop(0, ns, drained, 0)
-
-        @pl.when(has_right)
-        def _(p=p):
-            own_right(p).wait_send()
-
-        @pl.when(has_left)
-        def _(p=p):
-            own_left(p).wait_send()
-
-    for d, j, to_d, slot in ((0, 0, 1, 0), (0, 1, 2, 1), (0, 1, 1, 2), (0, 0, 2, 3), (1, 0, 2, 4), (2, 1, 1, 5)):
-        row_send(d, j, to_d, slot).wait_send()
-    for to_d in range(1, 3):
-        for i in range(4):
-            own_out(to_d, i).wait_send()
-        relay_out(3 - to_d, to_d).wait_send()
-    for i in range(2):
-        assist(i).wait_send()
-    for d in range(nf):
-        twin(d).wait_send()
-        if d:
-            leak_send(d).wait_send()
-            for j in range(2):
-                mixed_send(d, j).wait_send()
-    for i in range(len(plan)):
-        share(i).wait_send()
+        if i >= lag:
+            finish(i - lag, *plan[i - lag][:2])
+    for i in range(len(plan) - lag, len(plan)):
+        finish(i, *plan[i][:2])
+
+
+    def drained(ref, sem):
+        pltpu.make_async_copy(ref, ref, sem).wait()
+
+    @pl.when(inner)
+    def _():
+        drained(wg, zs.at[0])
+
+    own_rows = wg.at[pl.ds(pl.multiple_of(s * kd, kd), kd), :]
+
+    @pl.when(s == 0)
+    def _():
+        drained(own_rows, zs.at[0])
+
+    @pl.when(has_left)
+    def _():
+        drained(own_rows, zsl.at[0])
+
+    drained(rows.at[pl.ds(0, 3), pl.ds(0, half), :], rs.at[0])
+    drained(rows.at[:, pl.ds(0, half), :], ts.at[0])
+    drained(others, ls.at[0])
+    drained(msend, xs.at[0])
+    drained(orecv, es.at[0])
+    drained(done, fin.at[0])
+
+    def quarters(side):
+        count = 2 * (8 * depth - taken[side]) + 8 * depth + 2 * taken[1 - side]
+        drained(wo.at[:, pl.ds(0, count // 16), :], os_.at[0])
+
+    by_side(quarters)
 
     @pl.when(has_right)
     def _():
-        for d in range(nf):
-            state_copy(d).wait_send()
-            rim_copy(d).wait_send()
+        drained(sout, ss.at[0])
+        drained(brim, ms.at[0])
 
 
 def body(ns, nf, tokens, norm_gain, w0, w1, w2, w3, w4, conv_taps, floor_gate, leak, head_gain, cow, how):
@@ -519,7 +605,6 @@
     wide = w0.shape[1] // nf
     assert heads == nf and nf == 4 and floor_gate.shape[0] == heads * wide and ns % 2 == 0
     taps = conv_taps.reshape(conv_taps.shape[0], nf, wide).transpose(1, 0, 2)
-    vm = pl.BlockSpec(memory_space=pltpu.VMEM)
     hbm = pl.BlockSpec(memory_space=pltpu.HBM)
     dma = pltpu.SemaphoreType.DMA
     depth, cols = cow.shape
@@ -535,6 +620,7 @@
         pltpu.VMEM((nf, length, 5 * wide), BF),
         pltpu.VMEM((nf, 2 * depth, cols), BF),
         pltpu.VMEM((nf, 16, wide), BF),
+        pltpu.VMEM((nf, 16, wide), BF),
         pltpu.VMEM((nf, length, wide), F32),
         pltpu.VMEM((nf, length, wide), F32),
         pltpu.VMEM((nf, length, wide), BF),
@@ -545,21 +631,22 @@
         pltpu.VMEM((nf, 8, length), F32),
         pltpu.VMEM((nf, length, wide), F32),
         pltpu.VMEM((nf, 8, length), F32),
-        pltpu.VMEM((nf, 2, length, wide), BF),
+        pltpu.VMEM((nf - 1, 2, length, wide), BF),
         pltpu.VMEM((length, 2 * depth), BF),
         pltpu.VMEM((2 * nf, length, cols // 2), F32),
         pltpu.VMEM((2 * nf, half, cols // 2), F32),
-        dma((6,)), dma((ns, 5)), dma((5,)), dma((ns, 5)), dma((5,)),
-        dma((6,)), dma((nf, 2)), dma((nf,)), dma((nf,)), dma((nf,)), dma((nf,)),
-        dma((2,)), dma((3, 4)), dma((nf, 4)), dma((3,)), dma((2,)),
-        dma((nf, 2)), dma((nf, 2)), dma((nf,)), dma((nf,)), dma((nf,)), dma((nf,)),
-        dma((2 * nf,)), dma((2 * nf,)),
+        pltpu.VMEM((half, width), BF),
+        dma((6,)), dma((1,)), dma((1,)), dma((ns, 5)), dma((5,)),
+        dma((1,)), dma((nf - 1, 2)), dma((1,)), dma((nf,)), dma((1,)), dma((1,)),
+        dma((1,)), dma((1,)), dma((3, 4)), dma((2,)), dma((2,)),
+        dma((1,)), dma((1,)), dma((1,)), dma((1,)), dma((1,)), dma((nf,)),
+        dma((1,)), dma((2 * nf,)), dma((1,)),
     ]
     return pl.pallas_call(
         functools.partial(kernel, ns, nf),
         out_shape=jax.ShapeDtypeStruct(tokens.shape, BF),
         in_specs=[hbm] * 13,
-        out_specs=vm,
+        out_specs=hbm,
         scratch_shapes=scratch,
         compiler_params=pltpu.CompilerParams(
             collective_id=0, has_side_effects=True, vmem_limit_bytes=60 * 2**20

time: 75.5 us -> 71.8 us (0.951)
  Pallas kernels: 73 us -> 69.5 us
    pallas_call x1, Pallas kernels: 73 us -> 69.5 us  [body(): pl.pallas_call(functools.partial(kernel, ns, nf), out_shape=jax.ShapeDtyp...]
where the time goes in v3:
time: 71.8 us; the launch traced here: 71.6 us
  Pallas kernels  69.5 us (97%)
  local copies, waits for them, and re-layouts  2.09 us (3%)
    pallas_call x1, Pallas kernels, body(): pl.pallas_call(functools.partial(kernel, ns, nf), out_shape=jax.ShapeDtyp...  69.5 us
    unnamed x1, local copies, waits for them, and re-layouts  2.09 us

profile of v3, /device:TPU:9, one launch (start us, length us, event | category | flops | bytes accessed | tf_op | source)
XLA Modules:
  0.0 71.6 jit_solution(2500708454232962492)
XLA Ops:
  0.0 69.5 %shard_map.127 = bf16[1,192,2048]{2,1,0:T(8,128)(2,1)} custom-call(bf16[1,192,2048]{2,1,0:T(8,128)(2,1)} %tok_h.1, f32[1,2048]{1,0:T(1,128)} %bitcast.9, bf16[512,512]{1,0:T(8,128)(2,1)} %w0.1, bf16[512,512]{1,0:T(8,128)(2,1)} %w1.1, bf16[512,512]{1,0:T(8,128)(2,1)} %w2.1, bf16[512,512]{1,0:T(8,128)(2,1)} %w3.1, bf16[512,512]{1,0:T(8,128)(2,1)} %w4.1, ...), custom_call_target="tpu_custom_call" | custom-call | tf_op jit(solution)/shard_map/pallas_call | solution.py:645
  69.5 2.1 %copy.15 = bf16[1,192,2048]{2,1,0:T(8,128)(2,1)} copy(bf16[1,192,2048]{2,1,0:T(8,128)(2,1)} %shard_map.127) | data formatting | bytes 1572864

commit v4 on v3

--- a/solution.py
+++ b/solution.py
@@ -18,10 +18,10 @@
 def kernel(
     ns, nf,
     tok_h, gain_h, w0, w1, w2, w3, w4, taps_h, floor_h, leak_h, hgain_h, cow, how,
-    out,
+    part, twin_part,
     tokv, gain, taps, floor, leak_t, hgain,
     rows, wg, y, wo, brim, rim, filt, inside, reach, states, sdecay, sin, sout,
-    lk, lcol, lrow, msend, mix, acc, orecv, done,
+    lk, lcol, lrow, msend, mix, shares,
     il, zs, zsl, zr, zloc, rs, rr, ts, tr, ls, lr, oloc, os_, or_, ov, zc, xs, xr, ms, mr, ss, sr, es, er, fin,
 ):
     s, f, t = lax.axis_index("sp"), lax.axis_index("fs"), lax.axis_index("tp")
@@ -57,48 +57,58 @@
     def oload(j):
         return pltpu.make_async_copy(outs[j], wo.at[0, pl.ds(j * depth, depth), :], oloc.at[0])
 
+    quarter = half // 2
+    pieces = [pl.ds(j * quarter, quarter) for j in range(2)]
     loads = [
         pltpu.make_async_copy(src, dst, il.at[i])
         for i, (src, dst) in enumerate(
-            ((tok_h.at[0], tokv), (gain_h, gain), (leak_h, leak_t), (taps_h, taps), (floor_h, floor), (hgain_h, hgain))
+            (
+                (tok_h.at[0, pieces[0]], tokv.at[pieces[0]]), (gain_h, gain), (tok_h.at[0, pieces[1]], tokv.at[pieces[1]]),
+                (leak_h, leak_t), (taps_h, taps), (floor_h, floor), (hgain_h, hgain),
+            )
         )
     ]
 
+    barrier = pltpu.get_barrier_semaphore()
+    for d in range(nf - 1, 0, -1):
+        pl.semaphore_signal(barrier, inc=1, device_id={"fs": f ^ d}, device_id_type=MESH)
+
+    @pl.when(has_left)
+    def _():
+        pl.semaphore_signal(barrier, inc=1, device_id={"sp": s - 1}, device_id_type=MESH)
+
+    @pl.when(has_right)
+    def _():
+        pl.semaphore_signal(barrier, inc=1, device_id={"sp": s + 1}, device_id_type=MESH)
+
+    pl.semaphore_signal(barrier, inc=1, device_id={"tp": other}, device_id_type=MESH)
+
+    for load in loads[:4]:
+        load.start()
     wload(0).start()
-    loads[0].start()
     wload(1).start()
-    for load in loads[1:]:
+    for load in loads[4:]:
         load.start()
     for p in range(2, np_):
         wload(p).start()
     for j in range(2):
         oload(j).start()
 
-    barrier = pltpu.get_barrier_semaphore()
-    for d in range(nf - 1, 0, -1):
-        pl.semaphore_signal(barrier, inc=1, device_id={"fs": f ^ d}, device_id_type=MESH)
-
-    @pl.when(has_left)
-    def _():
-        pl.semaphore_signal(barrier, inc=1, device_id={"sp": s - 1}, device_id_type=MESH)
-
-    @pl.when(has_right)
-    def _():
-        pl.semaphore_signal(barrier, inc=1, device_id={"sp": s + 1}, device_id_type=MESH)
-
-    pl.semaphore_signal(barrier, inc=1, device_id={"tp": other}, device_id_type=MESH)
-
-
-    for load in loads[:3]:
-        load.wait()
+
+    loads[3].wait()
     lk[0, pl.ds(0, leak_t.shape[0]), :] = leak_t[...]
-    x = tokv[...].astype(F32)
-    center = x - jnp.mean(x, axis=-1, keepdims=True)
-    spread = jnp.mean(center * center, axis=-1, keepdims=True)
-    rows[0, pl.ds(pl.multiple_of(t * half, half), half), :] = (
-        center * lax.rsqrt(spread + 1e-05) * gain[...]
-    ).astype(BF)
-
+
+    def normalize(j):
+        for load in loads[2 * j : 2 + j]:
+            load.wait()
+        x = tokv[pieces[j]].astype(F32)
+        center = x - jnp.mean(x, axis=-1, keepdims=True)
+        spread = jnp.mean(center * center, axis=-1, keepdims=True)
+        rows[0, pl.ds(pl.multiple_of(t * half + j * quarter, quarter), quarter), :] = (
+            center * lax.rsqrt(spread + 1e-05) * gain[...]
+        ).astype(BF)
+
+    normalize(0)
     ends = jnp.where(has_left, 1, 0) + jnp.where(has_right, 1, 0)
     pl.semaphore_wait(barrier, nf + ends)
 
@@ -158,8 +168,6 @@
         wload(p).wait()
         send_own(p, always)
 
-    quarter = half // 2
-
     def piece(d, j):
         return rows.at[d, pl.ds(pl.multiple_of(t * half + j * quarter, quarter), quarter), :]
 
@@ -184,6 +192,7 @@
     for d in range(1, nf):
         leak_send(d).start()
     row_send(0, 0, 1).start()
+    normalize(1)
     row_send(0, 1, 2).start()
     row_send(0, 1, 1).start()
     row_send(0, 0, 2).start()
@@ -243,24 +252,26 @@
     def third_lower(to_d):
         return own_out(to_d, 2, lower)
 
-    taken = (depth, depth // 2)
-
-    def fourth(to_d, side):
-        return own_out(to_d, 3, (taken[side], 2 * depth - taken[side]))
-
-    def swap(d, side):
-        q, part = order(d, 0), (0, taken[1 - side])
+    def taken(side, core):
+        return depth * (3 - 2 * core) // (2 + 2 * side)
+
+    def fourth(to_d, side, core):
+        return own_out(to_d, 3, (taken(side, core), 2 * depth - taken(side, core)))
+
+    def swap(d, side, core):
+        q, part = order(d, 0), (0, taken(1 - side, core))
         return remote(opiece(d, q, part), opiece(d, q, part), os_.at[0], zc.at[d - 1], sp=mate)
 
-    def swapped(d, side):
-        q, part = order(d, 3), (0, taken[side])
+    def swapped(d, side, core):
+        q, part = order(d, 3), (0, taken(side, core))
         remote(opiece(d, q, part), opiece(d, q, part), os_.at[0], zc.at[d - 1], sp=mate).wait_recv()
 
     def by_side(work):
         for side in range(2):
-            @pl.when(odd == side)
-            def _(side=side):
-                work(side)
+            for core in range(2):
+                @pl.when((odd == side) & (t == core))
+                def _(side=side, core=core):
+                    work(side, core)
 
     def relay_out(d, to_d):
         q = order(d, 0)
@@ -338,7 +349,7 @@
 
         lax.fori_loop(first, last, one, 0)
 
-    for load in loads[3:]:
+    for load in loads[4:]:
         load.wait()
     twin_arrived(0)
     zready(0)
@@ -412,8 +423,11 @@
         return remote(brim, rim, ms.at[0], mr.at[0], sp=s + 1)
 
     def swaps(side):
-        for d in (1, 2):
-            swap(d, side).start()
+        for core in range(2):
+            @pl.when(t == core)
+            def _(core=core):
+                for d in (1, 2):
+                    swap(d, side, core).start()
 
     def signal():
         zready(3)
@@ -496,43 +510,38 @@
     for to_d in (1, 2):
         third_lower(to_d).start()
 
-    def fourths(side):
+    def fourths(side, core):
         for to_d in (1, 2):
-            fourth(to_d, side).start()
+            fourth(to_d, side, core).start()
 
     by_side(fourths)
 
-
-    def share(i):
-        return remote(
-            acc.at[i, pl.ds(pl.multiple_of(other * half, half), half), :], orecv.at[i], es.at[0], er.at[i], tp=other
-        )
 
     mixed = remote(msend, msend, xs.at[0], xr.at[0], fs=f ^ 1)
     mixed.wait_recv()
 
-    def begin(i, d, c):
-        co = pl.ds(pl.multiple_of(c * 2 * pw, 2 * pw), 2 * pw)
-        acc[i] = jnp.dot(mix[...], wo[d, :, co], preferred_element_type=F32)
-        share(i).start()
-
-    def finish(i, d, c):
-        share(i).wait_recv()
-        at = pl.ds(pl.multiple_of((f ^ d) * cols + c * 2 * pw, 2 * pw), 2 * pw)
-        done[:, at] = (acc[i, pl.ds(pl.multiple_of(t * half, half), half), :] + orecv[i]).astype(BF)
-        store(i, d, c).start()
-
-    def store(i, d, c):
-        at = pl.ds(pl.multiple_of((f ^ d) * cols + c * 2 * pw, 2 * pw), 2 * pw)
-        return pltpu.make_async_copy(done.at[:, at], out.at[0, :, at], fin.at[0])
+    def rows_of(core):
+        return pl.ds(pl.multiple_of(core * half, half), half)
+
+    def finish(chunks):
+        spans = []
+        for d, c in chunks:
+            co = pl.ds(pl.multiple_of(c * 2 * pw, 2 * pw), 2 * pw)
+            at = pl.ds(pl.multiple_of((f ^ d) * cols + c * 2 * pw, 2 * pw), 2 * pw)
+            shares[:, at] = jnp.dot(mix[...], wo[d, :, co], preferred_element_type=F32).astype(BF)
+            spans.append(at)
+        for at in spans:
+            remote(shares.at[rows_of(other), at], twin_part.at[0, :, at], es.at[0], er.at[0], tp=other).start()
+        for at in spans:
+            pltpu.make_async_copy(shares.at[rows_of(t), at], part.at[0, :, at], fin.at[0]).start()
 
     def last_quarters(d):
         third_upper(d).wait_recv()
         out_arrived(d, order(d, 2), lower)
 
-        def rest(side):
-            swapped(d, side)
-            out_arrived(d, order(d, 3), (taken[side], 2 * depth - taken[side]))
+        def rest(side, core):
+            swapped(d, side, core)
+            out_arrived(d, order(d, 3), (taken(side, core), 2 * depth - taken(side, core)))
 
         by_side(rest)
 
@@ -540,25 +549,13 @@
         for q in (2 - 2 * odd, 3 - 2 * odd):
             out_arrived(3, q)
 
-    lag = 3
-    plan = [
-        (0, odd, None),
-        (0, 1 - odd, None),
-        (1, odd, lambda d: out_arrived(d, order(d, 1))),
-        (2, odd, lambda d: out_arrived(d, order(d, 1))),
-        (3, odd, None),
-        (1, 1 - odd, last_quarters),
-        (2, 1 - odd, last_quarters),
-        (3, 1 - odd, assisted),
-    ]
-    for i, (d, c, ready) in enumerate(plan):
-        if ready:
-            ready(d)
-        begin(i, d, c)
-        if i >= lag:
-            finish(i - lag, *plan[i - lag][:2])
-    for i in range(len(plan) - lag, len(plan)):
-        finish(i, *plan[i][:2])
+    for d in (1, 2):
+        out_arrived(d, order(d, 1))
+    finish([(0, odd), (0, 1 - odd), (1, odd), (2, odd), (3, odd)])
+    for d in (1, 2):
+        last_quarters(d)
+    assisted(3)
+    finish([(1, 1 - odd), (2, 1 - odd), (3, 1 - odd)])
 
 
     def drained(ref, sem):
@@ -582,11 +579,9 @@
     drained(rows.at[:, pl.ds(0, half), :], ts.at[0])
     drained(others, ls.at[0])
     drained(msend, xs.at[0])
-    drained(orecv, es.at[0])
-    drained(done, fin.at[0])
-
-    def quarters(side):
-        count = 2 * (8 * depth - taken[side]) + 8 * depth + 2 * taken[1 - side]
+
+    def quarters(side, core):
+        count = 2 * (8 * depth - taken(side, core)) + 8 * depth + 2 * taken(1 - side, core)
         drained(wo.at[:, pl.ds(0, count // 16), :], os_.at[0])
 
     by_side(quarters)
@@ -595,6 +590,11 @@
     def _():
         drained(sout, ss.at[0])
         drained(brim, ms.at[0])
+
+    mine = shares.at[rows_of(t), :]
+    drained(mine, es.at[0])
+    drained(mine, fin.at[0])
+    drained(mine, er.at[0])
 
 
 def body(ns, nf, tokens, norm_gain, w0, w1, w2, w3, w4, conv_taps, floor_gate, leak, head_gain, cow, how):
@@ -633,20 +633,18 @@
         pltpu.VMEM((nf, 8, length), F32),
         pltpu.VMEM((nf - 1, 2, length, wide), BF),
         pltpu.VMEM((length, 2 * depth), BF),
-        pltpu.VMEM((2 * nf, length, cols // 2), F32),
-        pltpu.VMEM((2 * nf, half, cols // 2), F32),
-        pltpu.VMEM((half, width), BF),
-        dma((6,)), dma((1,)), dma((1,)), dma((ns, 5)), dma((5,)),
+        pltpu.VMEM((length, width), BF),
+        dma((7,)), dma((1,)), dma((1,)), dma((ns, 5)), dma((5,)),
         dma((1,)), dma((nf - 1, 2)), dma((1,)), dma((nf,)), dma((1,)), dma((1,)),
         dma((1,)), dma((1,)), dma((3, 4)), dma((2,)), dma((2,)),
         dma((1,)), dma((1,)), dma((1,)), dma((1,)), dma((1,)), dma((nf,)),
-        dma((1,)), dma((2 * nf,)), dma((1,)),
+        dma((1,)), dma((1,)), dma((1,)),
     ]
-    return pl.pallas_call(
+    part, twin_part = pl.pallas_call(
         functools.partial(kernel, ns, nf),
-        out_shape=jax.ShapeDtypeStruct(tokens.shape, BF),
+        out_shape=[jax.ShapeDtypeStruct(tokens.shape, BF)] * 2,
         in_specs=[hbm] * 13,
-        out_specs=hbm,
+        out_specs=[hbm] * 2,
         scratch_shapes=scratch,
         compiler_params=pltpu.CompilerParams(
             collective_id=0, has_side_effects=True, vmem_limit_bytes=60 * 2**20
@@ -655,6 +653,7 @@
         tokens, norm_gain[None], w0, w1, w2, w3, w4, taps, floor_gate.reshape(heads, 1, wide),
         leak[0].T, head_gain[None], cow, how,
     )
+    return (part.astype(F32) + twin_part.astype(F32)).astype(BF)
 
 
 def solution(mesh):

time: 71.8 us -> 70.9 us (0.987)
  other arithmetic: 0 us -> 2.52 us
  local copies, waits for them, and re-layouts: 2.09 us -> 0 us
  Pallas kernels: 69.5 us -> 68.2 us
    convert_element_type x0 -> x1, other arithmetic: none -> 2.52 us  [body(): return (part.astype(F32) + twin_part.astype(F32)).astype(BF)]
    unnamed x1 -> x0, local copies, waits for them, and re-layouts: 2.09 us -> none
    pallas_call x1, Pallas kernels: 69.5 us -> 68.2 us  [body(): pl.pallas_call(functools.partial(kernel, ns, nf), out_shape=[jax.ShapeDty...]
where the time goes in v4:
time: 70.9 us; the launch traced here: 70.7 us
  Pallas kernels  68.2 us (96%)
  other arithmetic  2.52 us (4%)
    pallas_call x1, Pallas kernels, body(): pl.pallas_call(functools.partial(kernel, ns, nf), out_shape=[jax.ShapeDty...  68.2 us
    convert_element_type x1, other arithmetic, body(): return (part.astype(F32) + twin_part.astype(F32)).astype(BF)  2.52 us

profile of v4, /device:TPU:9, one launch (start us, length us, event | category | flops | bytes accessed | tf_op | source)
XLA Modules:
  0.0 70.7 jit_solution(7660669990055423125)
XLA Ops:
  0.0 68.2 %shard_map.127 = (bf16[1,192,2048]{2,1,0:T(8,128)(2,1)}, bf16[1,192,2048]{2,1,0:T(8,128)(2,1)}) custom-call(bf16[1,192,2048]{2,1,0:T(8,128)(2,1)} %tok_h.1, f32[1,2048]{1,0:T(1,128)} %bitcast.9, bf16[512,512]{1,0:T(8,128)(2,1)} %w0.1, bf16[512,512]{1,0:T(8,128)(2,1)} %w1.1, bf16[512,512]{1,0:T(8,128)(2,1)} %w2.1, bf16[512,512]{1,0:T(8,128)(2,1)} %w3.1, ...), custom_call_target="tpu_custom_call" | custom-call | tf_op jit(solution)/shard_map/pallas_call | solution.py:643
  68.2 2.5 %add_convert_fusion = bf16[1,192,2048]{2,1,0:T(8,128)(2,1)} fusion(bf16[1,192,2048]{2,1,0:T(8,128)(2,1)} %get-tuple-element.8, bf16[1,192,2048]{2,1,0:T(8,128)(2,1)} %get-tuple-element.7), kind=kLoop, calls=%fused_computation | loop fusion | flops 1572864 | bytes 2359296 | tf_op jit(solution)/shard_map/convert_element_type | solution.py:656

commit v5 on v4

--- a/solution.py
+++ b/solution.py
@@ -253,7 +253,7 @@
         return own_out(to_d, 2, lower)
 
     def taken(side, core):
-        return depth * (3 - 2 * core) // (2 + 2 * side)
+        return depth * ((6, 4), (2, 1))[core][side] // 4
 
     def fourth(to_d, side, core):
         return own_out(to_d, 3, (taken(side, core), 2 * depth - taken(side, core)))
@@ -365,8 +365,8 @@
     row_arrived(3, 1)
     twin(3).start()
     many(local, 0, 3)
+    zhop(2, 3)
     zhop(1, 4)
-    zhop(2, 3)
     zhop(2, 4)
     twin_arrived(3)
     project(3, 1, 0, 2)

time: 70.9 us -> 70.6 us (level)
  no operation moved by 1% of the time
where the time goes in v5:
time: 70.6 us; the launch traced here: 70.4 us
  Pallas kernels  67.8 us (96%)
  other arithmetic  2.52 us (4%)
    pallas_call x1, Pallas kernels, body(): pl.pallas_call(functools.partial(kernel, ns, nf), out_shape=[jax.ShapeDty...  67.8 us
    convert_element_type x1, other arithmetic, body(): return (part.astype(F32) + twin_part.astype(F32)).astype(BF)  2.52 us

profile of v5, /device:TPU:9, one launch (start us, length us, event | category | flops | bytes accessed | tf_op | source)
XLA Modules:
  0.0 70.4 jit_solution(14699402506361467561)
XLA Ops:
  0.0 67.8 %shard_map.127 = (bf16[1,192,2048]{2,1,0:T(8,128)(2,1)}, bf16[1,192,2048]{2,1,0:T(8,128)(2,1)}) custom-call(bf16[1,192,2048]{2,1,0:T(8,128)(2,1)} %tok_h.1, f32[1,2048]{1,0:T(1,128)} %bitcast.9, bf16[512,512]{1,0:T(8,128)(2,1)} %w0.1, bf16[512,512]{1,0:T(8,128)(2,1)} %w1.1, bf16[512,512]{1,0:T(8,128)(2,1)} %w2.1, bf16[512,512]{1,0:T(8,128)(2,1)} %w3.1, ...), custom_call_target="tpu_custom_call" | custom-call | tf_op jit(solution)/shard_map/pallas_call | solution.py:643
  67.9 2.5 %add_convert_fusion = bf16[1,192,2048]{2,1,0:T(8,128)(2,1)} fusion(bf16[1,192,2048]{2,1,0:T(8,128)(2,1)} %get-tuple-element.8, bf16[1,192,2048]{2,1,0:T(8,128)(2,1)} %get-tuple-element.7), kind=kLoop, calls=%fused_computation | loop fusion | flops 1572864 | bytes 2359296 | tf_op jit(solution)/shard_map/convert_element_type | solution.py:656

commit v6 on v5

--- a/solution.py
+++ b/solution.py
@@ -253,7 +253,7 @@
         return own_out(to_d, 2, lower)
 
     def taken(side, core):
-        return depth * ((6, 4), (2, 1))[core][side] // 4
+        return depth * ((5, 4), (2, 1))[core][side] // 4
 
     def fourth(to_d, side, core):
         return own_out(to_d, 3, (taken(side, core), 2 * depth - taken(side, core)))

time: 70.6 us -> 70.6 us (level)
  no operation moved by 1% of the time
where the time goes in v6:
time: 70.6 us; the launch traced here: 70.4 us
  Pallas kernels  67.8 us (96%)
  other arithmetic  2.52 us (4%)
    pallas_call x1, Pallas kernels, body(): pl.pallas_call(functools.partial(kernel, ns, nf), out_shape=[jax.ShapeDty...  67.8 us
    convert_element_type x1, other arithmetic, body(): return (part.astype(F32) + twin_part.astype(F32)).astype(BF)  2.52 us

profile of v6, /device:TPU:9, one launch (start us, length us, event | category | flops | bytes accessed | tf_op | source)
XLA Modules:
  0.0 70.4 jit_solution(8871180489767779716)
XLA Ops:
  0.0 67.8 %shard_map.127 = (bf16[1,192,2048]{2,1,0:T(8,128)(2,1)}, bf16[1,192,2048]{2,1,0:T(8,128)(2,1)}) custom-call(bf16[1,192,2048]{2,1,0:T(8,128)(2,1)} %tok_h.1, f32[1,2048]{1,0:T(1,128)} %bitcast.9, bf16[512,512]{1,0:T(8,128)(2,1)} %w0.1, bf16[512,512]{1,0:T(8,128)(2,1)} %w1.1, bf16[512,512]{1,0:T(8,128)(2,1)} %w2.1, bf16[512,512]{1,0:T(8,128)(2,1)} %w3.1, ...), custom_call_target="tpu_custom_call" | custom-call | tf_op jit(solution)/shard_map/pallas_call | solution.py:643
  67.9 2.5 %add_convert_fusion = bf16[1,192,2048]{2,1,0:T(8,128)(2,1)} fusion(bf16[1,192,2048]{2,1,0:T(8,128)(2,1)} %get-tuple-element.8, bf16[1,192,2048]{2,1,0:T(8,128)(2,1)} %get-tuple-element.7), kind=kLoop, calls=%fused_computation | loop fusion | flops 1572864 | bytes 2359296 | tf_op jit(solution)/shard_map/convert_element_type | solution.py:656
